TPU v7x, 32 devices: a whole 2x2x4 slice. The times are simulated.
32 devices in a mesh: sp: 8 (over z, y), tp: 4 (over x, core).
Axes of the slice: x: 2, y: 2, z: 4, core: 2. Of those that a mesh axis runs over, the one named last changes fastest.
Arguments:
- tokens: bfloat16 [8192, 2048], P('sp', 'tp'), may hold values from -600 to 600, as said below
- norm_gain: float32 [2048], replicated, may hold values from 0.1 to 1.9
- w_query: bfloat16 [2048, 1024], P(None, 'tp'), may hold values from -0.125 to 0.125
- w_forget_fwd: bfloat16 [2048, 1024], P(None, 'tp'), may hold values from -0.125 to 0.125
- w_forget_bwd: bfloat16 [2048, 1024], P(None, 'tp'), may hold values from -0.125 to 0.125
- w_value: bfloat16 [2048, 1024], P(None, 'tp'), may hold values from -0.125 to 0.125
- w_gate: bfloat16 [2048, 1024], P(None, 'tp'), may hold values from -0.125 to 0.125
- w_pool_in: bfloat16 [2048, 1024], P(None, 'tp'), may hold values from -0.125 to 0.125
- forget_gap: float32 [2, 1024], P(None, 'tp'), may hold values from 0 to 0.06
- added_log_retention: float32 [8192, 8], P('sp', 'tp'), may hold values from -2.1 to 0
- initial_state: float32 [2, 8, 128, 128], P(None, 'tp'), may hold values from -0.18 to 0.18
- head_gain: float32 [1024], P('tp'), may hold values from 0.1 to 1.9
- pool_mix: bfloat16 [4, 256, 256], P('tp'), may hold values from -0.375 to 0.375
- pool_gain: float32 [1024], P('tp'), may hold values from 0.1 to 1.9
- w_out_recur: bfloat16 [1024, 2048], P('tp'), may hold values from -0.125 to 0.125
- w_out_pool: bfloat16 [1024, 2048], P('tp'), may hold values from -0.125 to 0.125
Outputs:
- mixed_out: bfloat16 [8192, 2048], P(('sp', 'tp'))
Inputs may be any that keep to these rules, and one draw needn't show every extreme that they name: `tokens`: layer input with scales that differ between rows and between columns.
All inputs are finite; a program needn't handle non-finite values.
Results may differ from a plain program's by a relative error of at most 0.013.
Values may be sent and summed in bfloat16 or wider, within the bound.
A program may use at most 128 MiB of HBM per device.

v0:
```python
import functools

import jax
import jax.numpy as jnp
from jax import lax
from jax.experimental import pallas as pl
from jax.experimental.pallas import tpu as pltpu
from jax.sharding import PartitionSpec as P

DEPTH = 128
CHUNK = 128
EPSILON = 1e-06
MESH = pl.DeviceIdType.MESH
F32 = jnp.float32
BF16 = jnp.bfloat16
VMEM_LIMIT = 60 * 1024 * 1024
ANY = pl.BlockSpec(memory_space=pl.ANY)
VM = pl.BlockSpec(memory_space=pltpu.VMEM)


def dot(a, b):
    return jnp.dot(a, b, preferred_element_type=F32)


def dot_t(a, b):
    return lax.dot_general(a, b, (((1,), (1,)), ((), ())), preferred_element_type=F32)


def t_dot(a, b, precision=None):
    return lax.dot_general(
        a, b, (((0,), (0,)), ((), ())), preferred_element_type=F32, precision=precision
    )


def peers():
    me = lax.axis_index("tp")
    sibling = me + 1 - 2 * lax.rem(me, 2)
    across = lax.rem(me + 2, 4)
    return me, sibling, across, lax.rem(sibling + 2, 4)


def greet(*devices):
    barrier = pltpu.get_barrier_semaphore()
    for device in devices:
        pl.semaphore_signal(barrier, inc=1, device_id={"tp": device}, device_id_type=MESH)
    pl.semaphore_wait(barrier, len(devices))


def project_kernel(pieces, tokens, gain, *refs):
    weights, outs = refs[:6], refs[6:12]
    held, wide, acc, square, w_sem, sib_sem, x_send, x_recv, f_send, f_recv = refs[12:]
    me, sibling, across, opposite = peers()
    length, width = tokens.shape
    rows = length // pieces
    loads = [pltpu.make_async_copy(w, wide.at[i], w_sem.at[i]) for i, w in enumerate(weights)]
    for load in loads:
        load.start()
    greet(sibling, across)

    def crossing(i):
        at = pl.ds(i * rows, rows)
        return pltpu.make_async_remote_copy(
            tokens.at[at], held.at[1, at], x_send.at[i], x_recv.at[i],
            device_id={"tp": across}, device_id_type=MESH,
        )

    def relay(i):
        at = pl.ds(i * rows, rows)
        return pltpu.make_async_remote_copy(
            held.at[1, at], held.at[2, at], f_send.at[i], f_recv.at[i],
            device_id={"tp": sibling}, device_id_type=MESH,
        )

    beside = pltpu.make_async_remote_copy(
        tokens, held.at[0], sib_sem.at[0], sib_sem.at[1],
        device_id={"tp": sibling}, device_id_type=MESH,
    )
    for i in range(pieces):
        crossing(i).start()
    beside.start()

    def part(block, owner, at, first):
        columns = pl.ds(pl.multiple_of(owner * width, width), width)
        x = block.astype(F32)
        total = jnp.sum(x * x, axis=1, keepdims=True)
        normed = (x * gain[:, columns]).astype(BF16)
        square[at, :] = total if first else square[at, :] + total
        for j in range(6):
            y = dot(normed, wide[j, columns, :])
            acc[j, at, :] = y if first else acc[j, at, :] + y

    for load in loads:
        load.wait()

    def own(i, _):
        at = pl.ds(pl.multiple_of(i * rows, rows), rows)
        part(tokens[at, :], me, at, True)
        return 0

    lax.fori_loop(0, pieces, own, 0)
    beside.wait()

    def near(i, _):
        at = pl.ds(pl.multiple_of(i * rows, rows), rows)
        part(held[0, at, :], sibling, at, False)
        return 0

    lax.fori_loop(0, pieces, near, 0)
    features = width * 4

    def far(i, _):
        at = pl.ds(pl.multiple_of(i * rows, rows), rows)
        crossing(i).wait_recv()
        relay(i).start()
        part(held[1, at, :], across, at, False)
        relay(i).wait_recv()
        part(held[2, at, :], opposite, at, False)
        scale = lax.rsqrt(square[at, :] / features + EPSILON)
        for j in range(6):
            outs[j][at, :] = (acc[j, at, :] * scale).astype(BF16)
        return 0

    lax.fori_loop(0, pieces, far, 0)
    for i in range(pieces):
        crossing(i).wait_send()
        relay(i).wait_send()


def project(tokens, gain, weights):
    length, width = tokens.shape
    depth, columns = weights[0].shape
    pieces = 4
    return pl.pallas_call(
        functools.partial(project_kernel, pieces),
        out_shape=[jax.ShapeDtypeStruct((length, columns), BF16)] * 6,
        in_specs=[VM, VM] + [ANY] * 6,
        out_specs=[VM] * 6,
        scratch_shapes=[
            pltpu.VMEM((3, length, width), BF16),
            pltpu.VMEM((6, depth, columns), BF16),
            pltpu.VMEM((6, length, columns), F32),
            pltpu.VMEM((length, 1), F32),
            pltpu.SemaphoreType.DMA((6,)),
            pltpu.SemaphoreType.DMA((2,)),
            pltpu.SemaphoreType.DMA((pieces,)),
            pltpu.SemaphoreType.DMA((pieces,)),
            pltpu.SemaphoreType.DMA((pieces,)),
            pltpu.SemaphoreType.DMA((pieces,)),
        ],
        compiler_params=pltpu.CompilerParams(
            collective_id=0, has_side_effects=True, vmem_limit_bytes=VMEM_LIMIT
        ),
        name="project",
    )(tokens, gain, *weights)


def strides():
    count = lax.axis_size("sp")
    return [1 << k for k in range(count.bit_length()) if 1 << k < count]


def partner(d, stride):
    me, count = lax.axis_index("sp"), lax.axis_size("sp")
    above, below = me + stride < count, me >= stride
    return (above, me + stride, below) if d == 0 else (below, me - stride, above)


def meet():
    barrier = pltpu.get_barrier_semaphore()
    for stride in strides():
        for d in range(2):
            exists, target, _ = partner(d, stride)

            @pl.when(exists)
            def _():
                pl.semaphore_signal(
                    barrier, inc=1, device_id={"sp": target}, device_id_type=MESH
                )

    number = jnp.int32(0)
    for stride in strides():
        for d in range(2):
            exists, _, _ = partner(d, stride)
            number = number + jnp.where(exists, 1, 0)
    pl.semaphore_wait(barrier, number)


def edge_copy(d, pool_in, edge, e_send, e_recv):
    length, rim = pool_in.shape[0], edge.shape[1]
    _, target, _ = partner(d, 1)
    begin = length - rim if d == 0 else 0
    return pltpu.make_async_remote_copy(
        pool_in.at[pl.ds(begin, rim)], edge.at[d], e_send.at[d], e_recv.at[d],
        device_id={"sp": target}, device_id_type=MESH,
    )


def edges_start(pool_in, edge, e_send, e_recv):
    for d in range(2):
        exists, _, source = partner(d, 1)

        @pl.when(exists)
        def _():
            edge_copy(d, pool_in, edge, e_send, e_recv).start()

        @pl.when(jnp.logical_not(source))
        def _():
            edge[d] = jnp.zeros(edge.shape[1:], edge.dtype)


def edges_close(pool_in, edge, e_send, e_recv):
    for d in range(2):
        exists, _, source = partner(d, 1)

        @pl.when(source)
        def _():
            edge_copy(d, pool_in, edge, e_send, e_recv).wait_recv()

        @pl.when(exists)
        def _():
            edge_copy(d, pool_in, edge, e_send, e_recv).wait_send()


def scan_copy(k, d, stride, sent, landed, p_send, p_recv):
    _, target, _ = partner(d, stride)
    return pltpu.make_async_remote_copy(
        sent.at[k, d], landed.at[k, d], p_send.at[k, d], p_recv.at[k, d],
        device_id={"sp": target}, device_id_type=MESH,
    )


def scan_start(k, state, offset, sent, landed, before, before_keep, p_send, p_recv):
    stride, heads = strides()[k], state.shape[1]
    for d in range(2):
        exists, _, _ = partner(d, stride)

        @pl.when(exists)
        def _():
            for h in range(heads):
                lanes = slice(h * DEPTH, (h + 1) * DEPTH)
                keep = jnp.exp(offset[d, :, lanes])
                sent[k, d, h, :DEPTH, :] = (keep * before[d, h] + state[d, h]).astype(BF16)
                sent[k, d, h, DEPTH:, :] = jnp.broadcast_to(
                    keep * before_keep[d, :, lanes], (16, DEPTH)
                ).astype(BF16)
            scan_copy(k, d, stride, sent, landed, p_send, p_recv).start()


def scan_close(k, state, sent, landed, before, before_keep, p_send, p_recv):
    stride, heads = strides()[k], state.shape[1]
    for d in range(2):
        exists, _, source = partner(d, stride)

        @pl.when(source)
        def _():
            scan_copy(k, d, stride, sent, landed, p_send, p_recv).wait_recv()
            for h in range(heads):
                lanes = slice(h * DEPTH, (h + 1) * DEPTH)
                keep = before_keep[d, :, lanes]
                early = landed[k, d, h].astype(F32)
                before[d, h] = keep * early[:DEPTH] + before[d, h]
                before_keep[d, :, lanes] = keep * early[DEPTH : DEPTH + 1]

        @pl.when(exists)
        def _():
            scan_copy(k, d, stride, sent, landed, p_send, p_recv).wait_send()


def local_kernel(
    query_pre, forget_fwd, forget_bwd, value, gap, added, initial, pool_in,
    out, carried_fwd, carried_bwd, entering, padded,
    state, offset, chunk_state, chunk_keep, sent, landed, before, before_keep, edge,
    p_send, p_recv, e_send, e_recv, enters, runs, cols, starts, offsets,
):
    length, width = query_pre.shape
    heads = width // DEPTH
    count = length // CHUNK
    row = lax.broadcasted_iota(jnp.int32, (CHUNK, CHUNK), 0)
    col = lax.broadcasted_iota(jnp.int32, (CHUNK, CHUNK), 1)
    lower = row >= col
    upper = row <= col
    lower_f, upper_f = lower.astype(F32), upper.astype(F32)
    lower_2 = jnp.concatenate([lower_f, lower_f], axis=1).astype(BF16)
    upper_2 = jnp.concatenate([upper_f, upper_f], axis=1).astype(BF16)
    exact = lax.Precision.HIGHEST

    def gates(pre, gap_row, sums):
        enter = gap_row * (1.0 / (1.0 + jnp.exp(pre[...].astype(F32))))
        keep = jnp.log1p(-enter)
        high = keep.astype(BF16)
        low = (keep - high.astype(F32)).astype(BF16)
        return enter, dot(sums, jnp.concatenate([high, low], axis=0))

    meet()
    edges_start(pool_in, edge, e_send, e_recv)
    state[...] = jnp.zeros_like(state)
    offset[...] = jnp.zeros_like(offset)

    def ascend(c, _):
        at = pl.ds(pl.multiple_of(c * CHUNK, CHUNK), CHUNK)
        values = value[at, :]
        enter_f, run_f = gates(forget_fwd.at[at], gap[0:1, :], lower_2)
        enter_b, run_b = gates(forget_bwd.at[at], gap[1:2, :], upper_2)
        add = added[at, :]
        col_f = jnp.dot(lower_f, add, precision=exact, preferred_element_type=F32)
        col_b = jnp.dot(upper_f, add, precision=exact, preferred_element_type=F32)
        enters[0, at, :], enters[1, at, :] = enter_f, enter_b
        runs[0, at, :], runs[1, at, :] = run_f, run_b
        cols[0, at, :], cols[1, at, :] = col_f, col_b
        close_f, close_b = run_f[CHUNK - 1 : CHUNK, :], run_b[0:1, :]
        last_f, last_b = enter_f * jnp.exp(close_f - run_f), enter_b * jnp.exp(close_b - run_b)
        offsets[0, c] = offset[0]
        for h in range(heads):
            lanes = slice(h * DEPTH, (h + 1) * DEPTH)
            a_col, b_col = col_f[:, h : h + 1], col_b[:, h : h + 1]
            a_end, b_end = a_col[CHUNK - 1 : CHUNK, :], b_col[0:1, :]
            v = values[:, lanes]
            total_f = close_f[:, lanes] + a_end
            ends_f = (last_f[:, lanes] * jnp.exp(a_end - a_col)).astype(BF16)
            ends_b = (last_b[:, lanes] * jnp.exp(b_end - b_col)).astype(BF16)
            ends = t_dot(v, jnp.concatenate([ends_f, ends_b], axis=1))
            starts[c, h, :, :DEPTH] = state[0, h].astype(BF16)
            state[0, h] = jnp.exp(total_f) * state[0, h] + ends[:, :DEPTH]
            chunk_state[c, h] = ends[:, DEPTH:]
            chunk_keep[c, :, lanes] = close_b[:, lanes] + b_end
            offset[0, :, lanes] = offset[0, :, lanes] + total_f
        return 0

    lax.fori_loop(0, count, ascend, 0)

    def descend(i, _):
        c = count - 1 - i
        offsets[1, c] = offset[1]
        for h in range(heads):
            lanes = slice(h * DEPTH, (h + 1) * DEPTH)
            starts[c, h, :, DEPTH:] = state[1, h].astype(BF16)
            total = chunk_keep[c, :, lanes]
            state[1, h] = jnp.exp(total) * state[1, h] + chunk_state[c, h]
            offset[1, :, lanes] = offset[1, :, lanes] + total
        return 0

    lax.fori_loop(0, count, descend, 0)

    def output(c, _):
        at = pl.ds(pl.multiple_of(c * CHUNK, CHUNK), CHUNK)
        x = query_pre[at, :].astype(F32)
        query = x / (1.0 + jnp.exp(-x))
        values = value[at, :]
        run_f, run_b = runs[0, at, :], runs[1, at, :]
        col_f, col_b = cols[0, at, :], cols[1, at, :]
        add = added[at, :]
        row_f = t_dot(add, upper_f, exact)
        row_b = t_dot(add, lower_f, exact)
        q_f, q_b = query * jnp.exp(run_f), query * jnp.exp(run_b)
        e_f = (enters[0, at, :] * jnp.exp(-run_f)).astype(BF16)
        e_b = (enters[1, at, :] * jnp.exp(-run_b)).astype(BF16)
        for h in range(heads):
            lanes = slice(h * DEPTH, (h + 1) * DEPTH)
            a_col, b_col = col_f[:, h : h + 1], col_b[:, h : h + 1]
            fade_f = jnp.exp(jnp.where(lower, a_col - row_f[h : h + 1, :], -1e30))
            fade_b = jnp.exp(jnp.where(upper, b_col - row_b[h : h + 1, :], -1e30))
            weight = (
                dot_t(q_f[:, lanes].astype(BF16), e_f[:, lanes]) * fade_f
                + dot_t(q_b[:, lanes].astype(BF16), e_b[:, lanes]) * fade_b
            )
            reach_f = q_f[:, lanes] * jnp.exp(a_col)
            reach_b = q_b[:, lanes] * jnp.exp(b_col)
            reach = jnp.concatenate([reach_f, reach_b], axis=1).astype(BF16)
            out[at, lanes] = dot(weight.astype(BF16), values[:, lanes]) + dot_t(reach, starts[c, h])
            carried_fwd[at, lanes] = (reach_f * jnp.exp(offsets[0, c, :, lanes])).astype(BF16)
            carried_bwd[at, lanes] = (reach_b * jnp.exp(offsets[1, c, :, lanes])).astype(BF16)
        return 0

    before[...] = jnp.zeros_like(before)
    before_keep[...] = jnp.ones_like(before_keep)
    steps = len(strides())
    for k in range(steps):
        scan_start(k, state, offset, sent, landed, before, before_keep, p_send, p_recv)
        lax.fori_loop(k * count // steps, (k + 1) * count // steps, output, 0)
        scan_close(k, state, sent, landed, before, before_keep, p_send, p_recv)
    for h in range(heads):
        lanes = slice(h * DEPTH, (h + 1) * DEPTH)
        for d in range(2):
            s = before_keep[d, :, lanes] * initial[d, h].T + before[d, h]
            entering[h, :, d * DEPTH : (d + 1) * DEPTH] = s.astype(BF16)
    rim = edge.shape[1]
    padded[rim : rim + length, :] = pool_in[...]
    edges_close(pool_in, edge, e_send, e_recv)
    padded[:rim, :] = edge[0]
    padded[rim + length :, :] = edge[1]


def local_pass(query_pre, forget_fwd, forget_bwd, value, gap, added, initial, pool_in, rim):
    length, width = query_pre.shape
    heads = width // DEPTH
    count = length // CHUNK
    steps = len(strides())
    flat = jax.ShapeDtypeStruct((length, width), BF16)
    return pl.pallas_call(
        local_kernel,
        out_shape=[
            jax.ShapeDtypeStruct((length, width), F32), flat, flat,
            jax.ShapeDtypeStruct((heads, DEPTH, 2 * DEPTH), BF16),
            jax.ShapeDtypeStruct((length + 2 * rim, pool_in.shape[1]), BF16),
        ],
        in_specs=[VM] * 8,
        out_specs=[VM] * 5,
        scratch_shapes=[
            pltpu.VMEM((2, heads, DEPTH, DEPTH), F32),
            pltpu.VMEM((2, 1, width), F32),
            pltpu.VMEM((count, heads, DEPTH, DEPTH), F32),
            pltpu.VMEM((count, 1, width), F32),
            pltpu.VMEM((steps, 2, heads, DEPTH + 16, DEPTH), BF16),
            pltpu.VMEM((steps, 2, heads, DEPTH + 16, DEPTH), BF16),
            pltpu.VMEM((2, heads, DEPTH, DEPTH), F32),
            pltpu.VMEM((2, 1, width), F32),
            pltpu.VMEM((2, rim, pool_in.shape[1]), BF16),
            pltpu.SemaphoreType.DMA((steps, 2)),
            pltpu.SemaphoreType.DMA((steps, 2)),
            pltpu.SemaphoreType.DMA((2,)),
            pltpu.SemaphoreType.DMA((2,)),
            pltpu.VMEM((2, length, width), F32),
            pltpu.VMEM((2, length, width), F32),
            pltpu.VMEM((2, length, heads), F32),
            pltpu.VMEM((count, heads, DEPTH, 2 * DEPTH), BF16),
            pltpu.VMEM((2, count, 1, width), F32),
        ],
        compiler_params=pltpu.CompilerParams(
            collective_id=2, has_side_effects=True, vmem_limit_bytes=VMEM_LIMIT
        ),
        name="local",
    )(query_pre, forget_fwd, forget_bwd, value, gap, added, initial, pool_in)


def block_of(begin, rows, refs, scratch, places):
    (local, carried_fwd, carried_bwd, gate_pre, head_gain, padded, mix, pool_gain, w_recur, w_pool) = refs
    entering, = scratch
    rim, sequence, first_row, window = places
    width = local.shape[1]
    heads = width // DEPTH
    at = pl.ds(begin, rows)
    recur = []
    for h in range(heads):
        lanes = slice(h * DEPTH, (h + 1) * DEPTH)
        reach = jnp.concatenate([carried_fwd[at, lanes], carried_bwd[at, lanes]], axis=1)
        both = local[at, lanes] + dot_t(reach, entering[h])
        both = both * lax.rsqrt(jnp.mean(both * both, axis=1, keepdims=True) + EPSILON)
        gate = gate_pre[at, lanes].astype(F32)
        recur.append((both * head_gain[:, lanes] / (1.0 + jnp.exp(-gate))).astype(BF16))
    total = dot(jnp.concatenate(recur, axis=1), w_recur[...])
    span = rows + 2 * rim
    near = padded[pl.ds(begin, span), :]
    target = first_row + begin + lax.broadcasted_iota(jnp.int32, (rows, span), 0)
    source = first_row + begin - rim + lax.broadcasted_iota(jnp.int32, (rows, span), 1)
    low = target - window // 2
    inside = (source >= low) & (source < low + window) & (source >= 0) & (source < sequence)
    start = first_row + begin + lax.broadcasted_iota(jnp.int32, (rows, 1), 0) - window // 2
    number = jnp.minimum(start + window, sequence) - jnp.maximum(start, 0)
    sums = dot(inside.astype(F32).astype(BF16), near)
    mean = sums / number.astype(F32)
    diff = (mean - padded[pl.ds(begin + rim, rows), :].astype(F32)).astype(BF16)
    pooled = (dot(diff, mix[0]) * pool_gain[...]).astype(BF16)
    return total + dot(pooled, w_pool[...])


def finish_kernel(groups, rim, *refs):
    entering, shared, out = refs[0], refs[1:11], refs[11]
    (kept, given, taken, sent, landed, g_send, g_recv, x_send, x_recv) = refs[12:]
    me, sibling, across, opposite = peers()
    greet(sibling, across)
    length = shared[0].shape[0]
    share = length // 4
    rows = kept.shape[1]
    pieces = share // rows
    group = lax.axis_index("tp") * groups
    window = jnp.left_shift(jnp.int32(2), group)
    places = (rim, length * lax.axis_size("sp"), lax.axis_index("sp") * length, window)

    def beside(i):
        return pltpu.make_async_remote_copy(
            given.at[i], taken.at[i], g_send.at[i], g_recv.at[i],
            device_id={"tp": sibling}, device_id_type=MESH,
        )

    def crossing(i):
        return pltpu.make_async_remote_copy(
            sent.at[i], landed.at[i], x_send.at[i], x_recv.at[i],
            device_id={"tp": across}, device_id_type=MESH,
        )

    def partial(owner, p):
        begin = pl.multiple_of(owner * share + p * rows, rows)
        return block_of(begin, rows, shared, (entering,), places).astype(BF16)

    def away(p, _):
        given[p] = partial(opposite, p)
        beside(p).start()
        mine = partial(across, p)
        beside(p).wait_recv()
        sent[p] = (mine.astype(F32) + taken[p].astype(F32)).astype(BF16)
        crossing(p).start()
        return 0

    lax.fori_loop(0, pieces, away, 0)

    def home(p, _):
        given[pieces + p] = partial(sibling, p)
        beside(pieces + p).start()
        kept[p] = partial(me, p)
        return 0

    lax.fori_loop(0, pieces, home, 0)

    def close(p, _):
        beside(pieces + p).wait_recv()
        crossing(p).wait_recv()
        total = kept[p].astype(F32) + taken[pieces + p].astype(F32) + landed[p].astype(F32)
        out[pl.ds(pl.multiple_of(p * rows, rows), rows), :] = total.astype(BF16)
        return 0

    lax.fori_loop(0, pieces, close, 0)
    for i in range(pieces):
        crossing(i).wait_send()
    for i in range(2 * pieces):
        beside(i).wait_send()


def finish(entering, shared, rim):
    length = shared[0].shape[0]
    features = shared[-1].shape[1]
    share, rows = length // 4, 128
    pieces = share // rows
    return pl.pallas_call(
        functools.partial(finish_kernel, shared[6].shape[0], rim),
        out_shape=jax.ShapeDtypeStruct((share, features), BF16),
        in_specs=[VM] * 11,
        out_specs=VM,
        scratch_shapes=[
            pltpu.VMEM((pieces, rows, features), BF16),
            pltpu.VMEM((2 * pieces, rows, features), BF16),
            pltpu.VMEM((2 * pieces, rows, features), BF16),
            pltpu.VMEM((pieces, rows, features), BF16),
            pltpu.VMEM((pieces, rows, features), BF16),
            pltpu.SemaphoreType.DMA((2 * pieces,)),
            pltpu.SemaphoreType.DMA((2 * pieces,)),
            pltpu.SemaphoreType.DMA((pieces,)),
            pltpu.SemaphoreType.DMA((pieces,)),
        ],
        compiler_params=pltpu.CompilerParams(
            collective_id=1, has_side_effects=True, vmem_limit_bytes=VMEM_LIMIT
        ),
        name="finish",
    )(entering, *shared)


def shards(
    tokens, norm_gain, w_query, w_forget_fwd, w_forget_bwd, w_value, w_gate, w_pool_in,
    forget_gap, added_log_retention, initial_state, head_gain, pool_mix, pool_gain,
    w_out_recur, w_out_pool,
):
    weights = (w_query, w_forget_fwd, w_forget_bwd, w_value, w_gate, w_pool_in)
    query_pre, forget_fwd, forget_bwd, value, gate_pre, pool_in = project(
        tokens, norm_gain[None, :], weights
    )
    rim = 16
    local, carried_fwd, carried_bwd, entering, padded = local_pass(
        query_pre, forget_fwd, forget_bwd, value, forget_gap, added_log_retention,
        initial_state, pool_in, rim,
    )
    shared = (
        local, carried_fwd, carried_bwd, gate_pre, head_gain[None, :], padded,
        pool_mix, pool_gain[None, :], w_out_recur, w_out_pool,
    )
    return finish(entering, shared, rim)


def solution(mesh):
    in_specs = (
        P("sp", "tp"), P(), P(None, "tp"), P(None, "tp"), P(None, "tp"), P(None, "tp"),
        P(None, "tp"), P(None, "tp"), P(None, "tp"), P("sp", "tp"), P(None, "tp", None, None),
        P("tp"), P("tp", None, None), P("tp"), P("tp", None), P("tp", None),
    )
    out_specs = P(("sp", "tp"), None)
    return jax.shard_map(shards, mesh=mesh, in_specs=in_specs, out_specs=out_specs, check_vma=False)
```

profile of v0, /device:TPU:1, one launch (start us, length us, event | category | flops | bytes accessed | tf_op | source)
XLA Modules:
  0.0 94.5 jit_solution(2168593264794212377)
XLA Ops:
  0.0 1.7 %copy.17.added = f32[1024,2]{1,0:T(8,128)} copy(f32[1024,2]{0,1:T(2,128)} %param.25) | data formatting | bytes 16384 | tf_op args[9]
  1.7 31.6 %project.1 = (bf16[1024,256]{1,0:T(8,128)(2,1)}, bf16[1024,256]{1,0:T(8,128)(2,1)}, bf16[1024,256]{1,0:T(8,128)(2,1)}, bf16[1024,256]{1,0:T(8,128)(2,1)}, bf16[1...) custom-call(bf16[1024,512]{1,0:T(8,128)(2,1)} %tokens.1, f32[1,2048]{1,0:T(1,128)} %bitcast.3, bf16[2048,256]{1,0:T(8,128)(2,1)} %refs_0_.1, ...), custom_call_target="tpu_custom_call" | custom-call | tf_op jit(solution)/shard_map/project/pallas_call | solution.py:133
  33.3 27.0 %local.1 = (f32[1024,256]{1,0:T(8,128)}, bf16[1024,256]{1,0:T(8,128)(2,1)}, bf16[1024,256]{1,0:T(8,128)(2,1)}, bf16[2,128,256]{2,1,0:T(8,128)(2,1)}, bf16[1056,256]{1,0:T(8,128)(2,1)}) custom-call(bf16[1024,256]{1,0:T(8,128)(2,1)} %get-tuple-element.16.query_pre, bf16[1024,256]{1,0:T(8,128)(2,1)} %get-tuple-element.17.forget_fwd, ...), custom_call_target="tpu_custom_call" | custom-call | tf_op jit(solution)/shard_map/local/pallas_call | solution.py:399
  60.3 31.9 %finish.1 = bf16[256,2048]{1,0:T(8,128)(2,1)} custom-call(bf16[2,128,256]{2,1,0:T(8,128)(2,1)} %get-tuple-element.21.refs_0_, f32[1024,256]{1,0:T(8,128)} %get-tuple-element.22.refs_1_, bf16[1024,256]{1,0:T(8,128)(2,1)} %get-tuple-element.23.refs_2_, bf16[1024,256]{1,0:T(8,128)(2,1)} %get-tuple-element.24.refs_3_, ...), custom_call_target="tpu_custom_call" | custom-call | tf_op jit(solution)/shard_map/finish/pallas_call | solution.py:533
  92.2 2.3 %copy.19 = bf16[256,2048]{1,0:T(8,128)(2,1)} copy(bf16[256,2048]{1,0:T(8,128)(2,1)} %finish.1) | data formatting | bytes 2097152
where the time goes:
time: 95.1 us; the launch traced here: 94.5 us
  Pallas kernels  90.4 us (95%)
  local copies, waits for them, and re-layouts  4.02 us (4%)
    pallas_call x1, Pallas kernels, finish(): pl.pallas_call(functools.partial(finish_kernel, shared[6].shape[0], rim),...  31.9 us
    pallas_call x1, Pallas kernels, project(): pl.pallas_call(functools.partial(project_kernel, pieces), out_shape=[jax....  31.6 us
    pallas_call x1, Pallas kernels, local_pass(): pl.pallas_call(local_kernel, out_shape=[jax.ShapeDtypeStruct((length, wid...  27 us
    unnamed x2, local copies, waits for them, and re-layouts  4.02 us

commit v1 on v0

v1 whole, which is shorter than its diff:
```python
import functools

import jax
import jax.numpy as jnp
from jax import lax
from jax.experimental import pallas as pl
from jax.experimental.pallas import tpu as pltpu
from jax.sharding import PartitionSpec as P

DEPTH = 128
CHUNK = 128
EPSILON = 1e-06
RIM = 16
RING = 8
MESH = pl.DeviceIdType.MESH
F32 = jnp.float32
BF16 = jnp.bfloat16
VMEM_LIMIT = 62 * 1024 * 1024
ANY = pl.BlockSpec(memory_space=pl.ANY)
VM = pl.BlockSpec(memory_space=pltpu.VMEM)
EXACT = lax.Precision.HIGHEST


def dot(a, b, precision=None):
    return jnp.dot(a, b, preferred_element_type=F32, precision=precision)


def dot_t(a, b, precision=None):
    return lax.dot_general(
        a, b, (((1,), (1,)), ((), ())), preferred_element_type=F32, precision=precision
    )


def t_dot(a, b):
    return lax.dot_general(a, b, (((0,), (0,)), ((), ())), preferred_element_type=F32)


def peers():
    me = lax.axis_index("tp")
    sibling = me + 1 - 2 * lax.rem(me, 2)
    across = lax.rem(me + 2, 4)
    return me, sibling, across, lax.rem(sibling + 2, 4)


def strides():
    count = lax.axis_size("sp")
    return [1 << k for k in range(count.bit_length()) if 1 << k < count]


def partner(d, stride):
    me, count = lax.axis_index("sp"), lax.axis_size("sp")
    above, below = me + stride < count, me >= stride
    return (above, me + stride, below) if d == 0 else (below, me - stride, above)


def ring_size():
    return min(RING, lax.axis_size("sp"))


def ring_place():
    size = ring_size()
    me = lax.axis_index("sp")
    base, mine = me - lax.rem(me, size), lax.rem(me, size)
    place = jnp.where(lax.rem(mine, 2) == 0, mine // 2, size - 1 - mine // 2)

    def index(spot):
        spot = lax.rem(spot + size, size)
        return base + jnp.where(spot < size // 2, 2 * spot, 2 * (size - 1 - spot) + 1)

    return place, index(place + 1), index(place - 1)


def greet():
    barrier = pltpu.get_barrier_semaphore()
    _, sibling, across, opposite = peers()
    _, right, left = ring_place()
    for device in (sibling, across, opposite):
        pl.semaphore_signal(barrier, inc=1, device_id={"tp": device}, device_id_type=MESH)
    for device in (right, left):
        pl.semaphore_signal(barrier, inc=1, device_id={"sp": device}, device_id_type=MESH)
    number = jnp.int32(5)
    for stride in strides():
        for d in range(2):
            exists, target, _ = partner(d, stride)

            @pl.when(exists)
            def _():
                pl.semaphore_signal(
                    barrier, inc=1, device_id={"sp": target}, device_id_type=MESH
                )

            number = number + jnp.where(exists, 1, 0)
    pl.semaphore_wait(barrier, number)


def edge_copy(d, length, padded, e_send, e_recv):
    _, target, _ = partner(d, 1)
    begin, there = (length, 0) if d == 0 else (RIM, RIM + length)
    return pltpu.make_async_remote_copy(
        padded.at[pl.ds(begin, RIM)], padded.at[pl.ds(there, RIM)], e_send.at[d], e_recv.at[d],
        device_id={"sp": target}, device_id_type=MESH,
    )


def edge_start(d, length, padded, e_send, e_recv):
    exists, _, _ = partner(d, 1)

    @pl.when(exists)
    def _():
        edge_copy(d, length, padded, e_send, e_recv).start()


def edges_wait(length, padded, e_send, e_recv):
    for d in range(2):
        _, _, source = partner(d, 1)

        @pl.when(source)
        def _():
            edge_copy(d, length, padded, e_send, e_recv).wait_recv()


def scan_copy(k, d, stride, sent, landed, p_send, p_recv):
    _, target, _ = partner(d, stride)
    return pltpu.make_async_remote_copy(
        sent.at[k, d], landed.at[k, d], p_send.at[k, d], p_recv.at[k, d],
        device_id={"sp": target}, device_id_type=MESH,
    )


def scan_start(k, d, state, offset, sent, landed, before, before_keep, p_send, p_recv):
    stride, heads = strides()[k], state.shape[1]
    exists, _, _ = partner(d, stride)

    @pl.when(exists)
    def _():
        for h in range(heads):
            lanes = slice(h * DEPTH, (h + 1) * DEPTH)
            keep = jnp.exp(offset[d, :, lanes])
            sent[k, d, h, :DEPTH, :] = (keep * before[d, h] + state[d, h]).astype(BF16)
            sent[k, d, h, DEPTH:, :] = jnp.broadcast_to(
                keep * before_keep[d, :, lanes], (16, DEPTH)
            ).astype(BF16)
        scan_copy(k, d, stride, sent, landed, p_send, p_recv).start()


def scan_close(k, d, state, sent, landed, before, before_keep, p_send, p_recv):
    stride, heads = strides()[k], state.shape[1]
    _, _, source = partner(d, stride)

    @pl.when(source)
    def _():
        scan_copy(k, d, stride, sent, landed, p_send, p_recv).wait_recv()
        for h in range(heads):
            lanes = slice(h * DEPTH, (h + 1) * DEPTH)
            keep = before_keep[d, :, lanes]
            early = landed[k, d, h].astype(F32)
            before[d, h] = keep * early[:DEPTH] + before[d, h]
            before_keep[d, :, lanes] = keep * early[DEPTH : DEPTH + 1]


def mixer_kernel(groups, *refs):
    (h_tokens, h_gain, *h_weights) = refs[:8]
    (h_gap, h_added, h_initial, h_head, h_mix, h_scale, h_recur, h_pool) = refs[8:16]
    out = refs[16]
    (
        held, gain, wide, gap, added, initial, head_gain, mix, pool_gain, wfull,
        acc, square, cols, rows_of, turned, query_pre, value, gated, ent, runs, inner, reach,
        starts, offsets, chunk_state, chunk_keep, state, offset, padded,
        sent, landed, before, before_keep, given, taken, passed, brought, total,
        l_sem, s_sem, x_send, x_recv, f_send, f_recv, w_sem, b_sem, r_sem,
        rr_send, rr_recv, rl_send, rl_recv, p_send, p_recv, e_send, e_recv,
        a_send, a_recv, c_send, c_recv,
    ) = refs[17:]
    me, sibling, across, opposite = peers()
    length, width = held.shape[1:]
    columns = wide.shape[2]
    heads = columns // DEPTH
    count = length // CHUNK
    share = length // 4
    subs = share // CHUNK
    features = 4 * width
    depth = wfull.shape[1] // 2
    steps = len(strides())

    own_w = [
        pltpu.make_async_copy(h_recur, wfull.at[me, pl.ds(0, depth)], l_sem.at[0]),
        pltpu.make_async_copy(h_pool, wfull.at[me, pl.ds(depth, depth)], l_sem.at[1]),
    ]
    own_t = pltpu.make_async_copy(h_tokens, held.at[me], l_sem.at[2])
    small = [
        pltpu.make_async_copy(a, b, l_sem.at[3 + i])
        for i, (a, b) in enumerate((
            (h_gain, gain), (h_gap, gap), (h_added, added), (h_initial, initial),
            (h_head, head_gain), (h_mix, mix), (h_scale, pool_gain),
        ))
    ]
    loads = [
        pltpu.make_async_copy(w, wide.at[i], l_sem.at[10 + i]) for i, w in enumerate(h_weights)
    ]
    for copy in own_w + [own_t] + small + loads:
        copy.start()
    greet()

    size = ring_size()
    slab = 2 * depth // size
    half = slab // 2
    place, right, left = ring_place()
    rights, lefts = 2 * (size // 2), 2 * (size - 1 - size // 2)

    mine = pl.ds(pl.multiple_of(place * slab, slab), slab)
    w_across = pltpu.make_async_remote_copy(
        wfull.at[me, mine], wfull.at[me, mine], w_sem.at[0], w_sem.at[1],
        device_id={"tp": across}, device_id_type=MESH,
    )
    w_beside = pltpu.make_async_remote_copy(
        wfull.at[me], wfull.at[me], b_sem.at[0], b_sem.at[1],
        device_id={"tp": sibling}, device_id_type=MESH,
    )
    w_relay = pltpu.make_async_remote_copy(
        wfull.at[across], wfull.at[across], r_sem.at[0], r_sem.at[1],
        device_id={"tp": sibling}, device_id_type=MESH,
    )

    def ring_right(e):
        spot = lax.rem(place - e // 2 + size, size)
        at = pl.ds(pl.multiple_of(spot * slab + lax.rem(e, 2) * half, half), half)
        return pltpu.make_async_remote_copy(
            wfull.at[across, at], wfull.at[across, at], rr_send.at[e], rr_recv.at[e],
            device_id={"sp": right}, device_id_type=MESH,
        )

    def ring_left(e):
        spot = lax.rem(place + e // 2, size)
        at = pl.ds(pl.multiple_of(spot * slab + lax.rem(e, 2) * half, half), half)
        return pltpu.make_async_remote_copy(
            wfull.at[across, at], wfull.at[across, at], rl_send.at[e], rl_recv.at[e],
            device_id={"sp": left}, device_id_type=MESH,
        )

    def ring_turn(e):
        @pl.when(e < rights)
        def _():
            ring_right(e).wait_recv()

        @pl.when(e + 2 < rights)
        def _():
            ring_right(e + 2).start()

        @pl.when(e < lefts)
        def _():
            ring_left(e).wait_recv()

        @pl.when(e + 2 < lefts)
        def _():
            ring_left(e + 2).start()

    beside = pltpu.make_async_remote_copy(
        held.at[me], held.at[me], s_sem.at[0], s_sem.at[1],
        device_id={"tp": sibling}, device_id_type=MESH,
    )

    def piece(i):
        return pl.ds(pl.multiple_of(i * CHUNK, CHUNK), CHUNK)

    def crossing(i):
        return pltpu.make_async_remote_copy(
            held.at[me, piece(i)], held.at[me, piece(i)], x_send.at[i], x_recv.at[i],
            device_id={"tp": across}, device_id_type=MESH,
        )

    def relay(i):
        return pltpu.make_async_remote_copy(
            held.at[across, piece(i)], held.at[across, piece(i)], f_send.at[i], f_recv.at[i],
            device_id={"tp": sibling}, device_id_type=MESH,
        )

    for copy in own_w:
        copy.wait()
    w_across.start()
    own_t.wait()
    beside.start()
    for i in range(count):
        crossing(i).start()
    w_beside.start()
    for copy in small:
        copy.wait()

    row = lax.broadcasted_iota(jnp.int32, (CHUNK, CHUNK), 0)
    col = lax.broadcasted_iota(jnp.int32, (CHUNK, CHUNK), 1)
    lower, upper = row >= col, row <= col
    lower_f, upper_f = lower.astype(F32), upper.astype(F32)
    lower_2 = jnp.concatenate([lower_f, lower_f], axis=1).astype(BF16)
    upper_2 = jnp.concatenate([upper_f, upper_f], axis=1).astype(BF16)

    def sums(c, _):
        add = added[:, piece(c)]
        cols[0, c] = dot_t(lower_f, add, EXACT)
        cols[1, c] = dot_t(upper_f, add, EXACT)
        rows_of[0, c] = dot(add, upper_f, EXACT)
        rows_of[1, c] = dot(add, lower_f, EXACT)
        return 0

    lax.fori_loop(0, count, sums, 0)
    for h in range(heads):
        for d in range(2):
            turned[h, :, d * DEPTH : (d + 1) * DEPTH] = initial[d, h].T
    state[...] = jnp.zeros_like(state)
    offset[...] = jnp.zeros_like(offset)
    before[...] = jnp.zeros_like(before)
    before_keep[...] = jnp.ones_like(before_keep)
    for d in range(2):
        _, _, source = partner(d, 1)
        begin = 0 if d == 0 else RIM + length

        @pl.when(jnp.logical_not(source))
        def _():
            padded[pl.ds(begin, RIM), :] = jnp.zeros((RIM, columns), BF16)

    pair = me // 2
    near, far = 2 * pair, 2 - 2 * pair

    def normed(first, at):
        parts, squares = [], 0.0
        for o in range(2):
            x = held[first + o, at, :].astype(F32)
            squares = squares + jnp.sum(x * x, axis=1, keepdims=True)
            lanes = pl.ds(pl.multiple_of((first + o) * width, width), width)
            parts.append((x * gain[:, lanes]).astype(BF16))
        return jnp.concatenate(parts, axis=1), squares

    def depth_of(first):
        return pl.ds(pl.multiple_of(first * width, 2 * width), 2 * width)

    for copy in loads:
        copy.wait()
    beside.wait_recv()

    def own(i, _):
        at = pl.ds(pl.multiple_of(i * share, share), share)
        x, squares = normed(near, at)
        square[at, :] = squares
        for j in range(6):
            acc[j, at, :] = dot(x, wide[j, depth_of(near), :])
        return 0

    lax.fori_loop(0, 4, own, 0)
    w_across.wait_recv()
    for e in range(2):
        ring_right(e).start()
        ring_left(e).start()

    def gates(pre, gap_row, sums):
        enter = gap_row * (1.0 / (1.0 + jnp.exp(pre)))
        keep = jnp.log1p(-enter)
        high = keep.astype(BF16)
        low = (keep - high.astype(F32)).astype(BF16)
        return enter, dot(sums, jnp.concatenate([high, low], axis=0))

    def local(c):
        at = piece(c)
        x = query_pre[at, :].astype(F32)
        query = x / (1.0 + jnp.exp(-x))
        q_f, q_b = query * jnp.exp(runs[0, at, :]), query * jnp.exp(runs[1, at, :])
        e_f, e_b = ent[0, at, :], ent[1, at, :]
        values = value[at, :]
        col_f, col_b = cols[0, c], cols[1, c]
        row_f, row_b = rows_of[0, c], rows_of[1, c]
        for h in range(heads):
            lanes = slice(h * DEPTH, (h + 1) * DEPTH)
            a_col, b_col = col_f[:, h : h + 1], col_b[:, h : h + 1]
            fade = jnp.exp(
                jnp.where(lower, a_col - row_f[h : h + 1, :], b_col - row_b[h : h + 1, :])
            )
            w_f = dot_t(q_f[:, lanes].astype(BF16), e_f[:, lanes])
            w_b = dot_t(q_b[:, lanes].astype(BF16), e_b[:, lanes])
            weight = (jnp.where(lower, w_f, 0.0) + jnp.where(upper, w_b, 0.0)) * fade
            inner[at, lanes] = dot(weight.astype(BF16), values[:, lanes])
            reach[h, at, :DEPTH] = (q_f[:, lanes] * jnp.exp(a_col)).astype(BF16)
            reach[h, at, DEPTH:] = (q_b[:, lanes] * jnp.exp(b_col)).astype(BF16)

    def step(i, _):
        at = piece(i)
        crossing(i).wait_recv()
        relay(i).start()

        @pl.when(i > 0)
        def _():
            ring_turn(i - 1)
            local(i - 1)

        relay(i).wait_recv()
        x, squares = normed(far, at)
        scale = lax.rsqrt((square[at, :] + squares) / features + EPSILON)

        def project(j):
            return ((acc[j, at, :] + dot(x, wide[j, depth_of(far), :])) * scale).astype(BF16)

        pre_f, pre_b, values = project(1), project(2), project(3)
        padded[pl.ds(pl.multiple_of(i * CHUNK + RIM, RIM), CHUNK), :] = project(5)

        @pl.when(i == 0)
        def _():
            edge_start(1, length, padded, e_send, e_recv)

        @pl.when(i == count - 1)
        def _():
            edge_start(0, length, padded, e_send, e_recv)

        value[at, :] = values
        enter_f, run_f = gates(pre_f.astype(F32), gap[0:1, :], lower_2)
        enter_b, run_b = gates(pre_b.astype(F32), gap[1:2, :], upper_2)
        runs[0, at, :], runs[1, at, :] = run_f, run_b
        e_f, e_b = enter_f * jnp.exp(-run_f), enter_b * jnp.exp(-run_b)
        ent[0, at, :], ent[1, at, :] = e_f.astype(BF16), e_b.astype(BF16)
        close_f, close_b = run_f[CHUNK - 1 : CHUNK, :], run_b[0:1, :]
        last_f, last_b = e_f * jnp.exp(close_f), e_b * jnp.exp(close_b)
        offsets[0, i] = offset[0]
        col_f, col_b = cols[0, i], cols[1, i]
        for h in range(heads):
            lanes = slice(h * DEPTH, (h + 1) * DEPTH)
            a_col, b_col = col_f[:, h : h + 1], col_b[:, h : h + 1]
            a_end, b_end = a_col[CHUNK - 1 : CHUNK, :], b_col[0:1, :]
            total_f = close_f[:, lanes] + a_end
            ends_f = (last_f[:, lanes] * jnp.exp(a_end - a_col)).astype(BF16)
            ends_b = (last_b[:, lanes] * jnp.exp(b_end - b_col)).astype(BF16)
            ends = t_dot(values[:, lanes], jnp.concatenate([ends_f, ends_b], axis=1))
            starts[i, h, :, :DEPTH] = state[0, h]
            state[0, h] = jnp.exp(total_f) * state[0, h] + ends[:, :DEPTH]
            chunk_state[i, h] = ends[:, DEPTH:]
            chunk_keep[i, :, lanes] = close_b[:, lanes] + b_end
            offset[0, :, lanes] = offset[0, :, lanes] + total_f
        query_pre[at, :] = project(0)
        gate = project(4).astype(F32)
        gated[at, :] = head_gain[...] / (1.0 + jnp.exp(-gate))
        return 0

    lax.fori_loop(0, count, step, 0)

    def descend(i, _):
        c = count - 1 - i
        offsets[1, c] = offset[1]
        for h in range(heads):
            lanes = slice(h * DEPTH, (h + 1) * DEPTH)
            starts[c, h, :, DEPTH:] = state[1, h]
            keep = chunk_keep[c, :, lanes]
            state[1, h] = jnp.exp(keep) * state[1, h] + chunk_state[c, h]
            offset[1, :, lanes] = offset[1, :, lanes] + keep
        return 0

    window = jnp.left_shift(jnp.int32(2), lax.axis_index("tp") * groups)
    sequence, first_row = length * lax.axis_size("sp"), lax.axis_index("sp") * length

    def pooled(owner):
        begin = pl.multiple_of(owner * share, share)
        span = share + 2 * RIM
        near_rows = padded[pl.ds(begin, span), :]
        target = first_row + begin + lax.broadcasted_iota(jnp.int32, (share, span), 0)
        source = first_row + begin - RIM + lax.broadcasted_iota(jnp.int32, (share, span), 1)
        low = target - window // 2
        inside = (source >= low) & (source < low + window) & (source >= 0) & (source < sequence)
        start = first_row + begin + lax.broadcasted_iota(jnp.int32, (share, 1), 0) - window // 2
        number = jnp.minimum(start + window, sequence) - jnp.maximum(start, 0)
        mean = dot(inside.astype(F32).astype(BF16), near_rows) / number.astype(F32)
        here = padded[pl.ds(pl.multiple_of(begin + RIM, RIM), share), :].astype(F32)
        return (dot((mean - here).astype(BF16), mix[0]) * pool_gain[...]).astype(BF16)

    others = (across, opposite, sibling)

    def pool_copy(k):
        return pltpu.make_async_remote_copy(
            passed.at[k], brought.at[me], a_send.at[k], a_recv.at[k],
            device_id={"tp": others[k]}, device_id_type=MESH,
        )

    def pool_away(k):
        passed[k] = pooled(others[k])
        pool_copy(k).start()

    def pool_home():
        brought[me] = pooled(me)

    def pool_first():
        edges_wait(length, padded, e_send, e_recv)
        pool_away(0)

    def ring_end():
        for e in range(count - 1, max(rights, lefts)):
            ring_turn(e)
        w_relay.start()

    scan = (sent, landed, before, before_keep, p_send, p_recv)
    fillers = [
        lambda: local(count - 1), pool_first, lambda: pool_away(1), ring_end,
        lambda: pool_away(2), pool_home,
    ]
    if steps:
        scan_start(0, 0, state, offset, *scan)
    lax.fori_loop(0, count, descend, 0)
    for k in range(steps):
        for d in range(2):
            if k or d:
                scan_start(k, d, state, offset, *scan)
        for filler in fillers[k * len(fillers) // steps : (k + 1) * len(fillers) // steps]:
            filler()
        for d in range(2):
            scan_close(k, d, state, *scan)
    if not steps:
        for filler in fillers:
            filler()
    for h in range(heads):
        for d in range(2):
            lanes = slice(d * DEPTH, (d + 1) * DEPTH)
            keep = before_keep[d, :, h * DEPTH : (h + 1) * DEPTH]
            turned[h, :, lanes] = keep * turned[h, :, lanes] + before[d, h]

    def finished(c):
        at = piece(c)
        for h in range(heads):
            lanes = slice(h * DEPTH, (h + 1) * DEPTH)
            ages = jnp.exp(
                jnp.concatenate([offsets[0, c, :, lanes], offsets[1, c, :, lanes]], axis=1)
            )
            enter = (starts[c, h] + ages * turned[h]).astype(BF16)
            both = inner[at, lanes] + dot_t(reach[h, at, :], enter)
            both = both * lax.rsqrt(jnp.mean(both * both, axis=1, keepdims=True) + EPSILON)
            yield lanes, (both * gated[at, lanes]).astype(BF16)

    def recur_copy(t):
        outward = t < 2 * subs
        there = jnp.where(outward, jnp.where(lax.rem(t, 2) == 0, across, opposite), sibling)
        sub = jnp.where(outward, t // 2, t - 2 * subs)
        at = piece(there * subs + sub)
        return there * subs + sub, pltpu.make_async_remote_copy(
            given.at[at], taken.at[me, piece(sub)], c_send.at[t], c_recv.at[t],
            device_id={"tp": there}, device_id_type=MESH,
        )

    def away(t, _):
        c, copy = recur_copy(t)
        for lanes, value_of in finished(c):
            given[piece(c), lanes] = value_of
        copy.start()
        return 0

    lax.fori_loop(0, 3 * subs, away, 0)

    def home(s, _):
        for lanes, value_of in finished(me * subs + s):
            taken[me, piece(s), lanes] = value_of
        return 0

    lax.fori_loop(0, subs, home, 0)

    tile = 512
    tiles = out.shape[1] // tile
    w_beside.wait_recv()
    w_relay.wait_recv()
    for k in range(3):
        pool_copy(k).wait_recv()
    for t in range(2 * subs, 3 * subs):
        recur_copy(jnp.int32(t))[1].wait_recv()

    def wide_part(j, _):
        lanes = pl.ds(pl.multiple_of(j * tile, tile), tile)
        y = dot(taken[me], wfull[me, :depth, lanes])
        y = y + dot(taken[sibling], wfull[sibling, :depth, lanes])
        for r in range(4):
            y = y + dot(brought[r], wfull[r, depth:, lanes])
        total[:, lanes] = y
        return 0

    lax.fori_loop(0, tiles, wide_part, 0)
    for s in range(subs):
        recur_copy(jnp.int32(2 * s))[1].wait_recv()
        recur_copy(jnp.int32(2 * s + 1))[1].wait_recv()
        at = slice(s * CHUNK, (s + 1) * CHUNK)
        for j in range(tiles):
            lanes = slice(j * tile, (j + 1) * tile)
            y = total[at, lanes] + dot(taken[across, at, :], wfull[across, :depth, lanes])
            y = y + dot(taken[opposite, at, :], wfull[opposite, :depth, lanes])
            out[at, lanes] = y.astype(BF16)

    w_across.wait_send()
    beside.wait_send()
    w_beside.wait_send()
    w_relay.wait_send()

    def sent_pieces(i, _):
        crossing(i).wait_send()
        relay(i).wait_send()
        return 0

    lax.fori_loop(0, count, sent_pieces, 0)
    for e in range(rights):
        ring_right(e).wait_send()
    for e in range(lefts):
        ring_left(e).wait_send()
    for d in range(2):
        exists, _, _ = partner(d, 1)

        @pl.when(exists)
        def _():
            edge_copy(d, length, padded, e_send, e_recv).wait_send()

    for k in range(steps):
        for d in range(2):
            exists, _, _ = partner(d, strides()[k])

            @pl.when(exists)
            def _():
                scan_copy(k, d, strides()[k], sent, landed, p_send, p_recv).wait_send()

    for k in range(3):
        pool_copy(k).wait_send()
    for t in range(3 * subs):
        recur_copy(jnp.int32(t))[1].wait_send()


def shards(
    tokens, norm_gain, w_query, w_forget_fwd, w_forget_bwd, w_value, w_gate, w_pool_in,
    forget_gap, added_log_retention, initial_state, head_gain, pool_mix, pool_gain,
    w_out_recur, w_out_pool,
):
    weights = (w_query, w_forget_fwd, w_forget_bwd, w_value, w_gate, w_pool_in)
    length, width = tokens.shape
    features, columns = w_query.shape
    heads = columns // DEPTH
    count = length // CHUNK
    share = length // 4
    subs = share // CHUNK
    depth, out_width = w_out_recur.shape
    steps = len(strides())
    size = ring_size()
    rights, lefts = 2 * (size // 2), 2 * (size - 1 - size // 2)
    dma = pltpu.SemaphoreType.DMA
    operands = (
        tokens, norm_gain[None, :], *weights, forget_gap, added_log_retention.T, initial_state,
        head_gain[None, :], pool_mix, pool_gain[None, :], w_out_recur, w_out_pool,
    )

    def like(array):
        return pltpu.VMEM(array.shape, array.dtype)

    return pl.pallas_call(
        functools.partial(mixer_kernel, pool_mix.shape[0]),
        out_shape=jax.ShapeDtypeStruct((share, out_width), BF16),
        in_specs=[ANY] * len(operands),
        out_specs=VM,
        scratch_shapes=[
            pltpu.VMEM((4, length, width), BF16),
            like(operands[1]),
            pltpu.VMEM((6, features, columns), BF16),
            like(operands[8]), like(operands[9]), like(operands[10]), like(operands[11]),
            like(operands[12]), like(operands[13]),
            pltpu.VMEM((4, 2 * depth, out_width), BF16),
            pltpu.VMEM((6, length, columns), F32),
            pltpu.VMEM((length, 1), F32),
            pltpu.VMEM((2, count, CHUNK, heads), F32),
            pltpu.VMEM((2, count, heads, CHUNK), F32),
            pltpu.VMEM((heads, DEPTH, 2 * DEPTH), F32),
            pltpu.VMEM((length, columns), BF16),
            pltpu.VMEM((length, columns), BF16),
            pltpu.VMEM((length, columns), F32),
            pltpu.VMEM((2, length, columns), BF16),
            pltpu.VMEM((2, length, columns), F32),
            pltpu.VMEM((length, columns), F32),
            pltpu.VMEM((heads, length, 2 * DEPTH), BF16),
            pltpu.VMEM((count, heads, DEPTH, 2 * DEPTH), F32),
            pltpu.VMEM((2, count, 1, columns), F32),
            pltpu.VMEM((count, heads, DEPTH, DEPTH), F32),
            pltpu.VMEM((count, 1, columns), F32),
            pltpu.VMEM((2, heads, DEPTH, DEPTH), F32),
            pltpu.VMEM((2, 1, columns), F32),
            pltpu.VMEM((length + 2 * RIM, columns), BF16),
            pltpu.VMEM((steps, 2, heads, DEPTH + 16, DEPTH), BF16),
            pltpu.VMEM((steps, 2, heads, DEPTH + 16, DEPTH), BF16),
            pltpu.VMEM((2, heads, DEPTH, DEPTH), F32),
            pltpu.VMEM((2, 1, columns), F32),
            pltpu.VMEM((length, columns), BF16),
            pltpu.VMEM((4, share, columns), BF16),
            pltpu.VMEM((3, share, columns), BF16),
            pltpu.VMEM((4, share, columns), BF16),
            pltpu.VMEM((share, out_width), F32),
            dma((16,)), dma((2,)), dma((count,)), dma((count,)), dma((count,)), dma((count,)),
            dma((2,)), dma((2,)), dma((2,)),
            dma((rights,)), dma((rights,)), dma((lefts,)), dma((lefts,)),
            dma((steps, 2)), dma((steps, 2)), dma((2,)), dma((2,)),
            dma((3,)), dma((3,)), dma((3 * subs,)), dma((3 * subs,)),
        ],
        compiler_params=pltpu.CompilerParams(
            collective_id=0, has_side_effects=True, vmem_limit_bytes=VMEM_LIMIT
        ),
        name="mixer",
    )(*operands)


def solution(mesh):
    in_specs = (
        P("sp", "tp"), P(), P(None, "tp"), P(None, "tp"), P(None, "tp"), P(None, "tp"),
        P(None, "tp"), P(None, "tp"), P(None, "tp"), P("sp", "tp"), P(None, "tp", None, None),
        P("tp"), P("tp", None, None), P("tp"), P("tp", None), P("tp", None),
    )
    out_specs = P(("sp", "tp"), None)
    return jax.shard_map(shards, mesh=mesh, in_specs=in_specs, out_specs=out_specs, check_vma=False)
```

time: 95.1 us -> 61.7 us (0.65)
  Pallas kernels: 90.4 us -> 59.2 us
  local copies, waits for them, and re-layouts: 4.02 us -> 2.3 us
    pallas_call x3 -> x1, Pallas kernels: 90.4 us -> 59.2 us  [shards(): pl.pallas_call(functools.partial(mixer_kernel, pool_mix.shape[0]), out_sh...]
    unnamed x2 -> x1, local copies, waits for them, and re-layouts: 4.02 us -> 2.3 us
where the time goes in v1:
time: 61.7 us; the launch traced here: 61.6 us
  Pallas kernels  59.2 us (96%)
  local copies, waits for them, and re-layouts  2.3 us (4%)
    pallas_call x1, Pallas kernels, shards(): pl.pallas_call(functools.partial(mixer_kernel, pool_mix.shape[0]), out_sh...  59.2 us
    unnamed x1, local copies, waits for them, and re-layouts  2.3 us

profile of v1, /device:TPU:1, one launch (start us, length us, event | category | flops | bytes accessed | tf_op | source)
XLA Modules:
  0.0 61.6 jit_solution(6735227983588257207)
XLA Ops:
  0.0 59.2 %mixer.1 = bf16[256,2048]{1,0:T(8,128)(2,1)} custom-call(bf16[1024,512]{1,0:T(8,128)(2,1)} %refs_0_.1, f32[1,2048]{1,0:T(1,128)} %bitcast.4, bf16[2048,256]{1,0:T(8,128)(2,1)} %refs_2_.1, bf16[2048,256]{1,0:T(8,128)(2,1)} %refs_3_.1, bf16[2048,256]{1,0:T(8,128)(2,1)} %refs_4_.1, bf16[2048,256]{1,0:T(8,128)(2,1)} %refs_5_.1, bf16[2048,256]{1,0:T(8,128)(2,1)} %refs_6_.1, ...), custom_call_target="tpu_custom_call" | custom-call | tf_op jit(solution)/shard_map/mixer/pallas_call | solution.py:644
  59.2 2.3 %copy.18 = bf16[256,2048]{1,0:T(8,128)(2,1)} copy(bf16[256,2048]{1,0:T(8,128)(2,1)} %mixer.1) | data formatting | bytes 2097152

commit v2 on v1

--- a/solution.py
+++ b/solution.py
@@ -119,43 +119,39 @@
             edge_copy(d, length, padded, e_send, e_recv).wait_recv()
 
 
-def scan_copy(k, d, stride, sent, landed, p_send, p_recv):
-    _, target, _ = partner(d, stride)
+def scan_copy(k, d, h, sent, landed, p_send, p_recv):
+    _, target, _ = partner(d, strides()[k])
     return pltpu.make_async_remote_copy(
-        sent.at[k, d], landed.at[k, d], p_send.at[k, d], p_recv.at[k, d],
+        sent.at[k, d, h], landed.at[k, d, h], p_send.at[k, d, h], p_recv.at[k, d, h],
         device_id={"sp": target}, device_id_type=MESH,
     )
 
 
-def scan_start(k, d, state, offset, sent, landed, before, before_keep, p_send, p_recv):
-    stride, heads = strides()[k], state.shape[1]
-    exists, _, _ = partner(d, stride)
+def scan_start(k, d, h, state, offset, sent, landed, before, before_keep, p_send, p_recv):
+    exists, _, _ = partner(d, strides()[k])
 
     @pl.when(exists)
     def _():
-        for h in range(heads):
-            lanes = slice(h * DEPTH, (h + 1) * DEPTH)
-            keep = jnp.exp(offset[d, :, lanes])
-            sent[k, d, h, :DEPTH, :] = (keep * before[d, h] + state[d, h]).astype(BF16)
-            sent[k, d, h, DEPTH:, :] = jnp.broadcast_to(
-                keep * before_keep[d, :, lanes], (16, DEPTH)
-            ).astype(BF16)
-        scan_copy(k, d, stride, sent, landed, p_send, p_recv).start()
-
-
-def scan_close(k, d, state, sent, landed, before, before_keep, p_send, p_recv):
-    stride, heads = strides()[k], state.shape[1]
-    _, _, source = partner(d, stride)
+        lanes = slice(h * DEPTH, (h + 1) * DEPTH)
+        keep = jnp.exp(offset[d, :, lanes])
+        sent[k, d, h, :DEPTH, :] = (keep * before[d, h] + state[d, h]).astype(BF16)
+        sent[k, d, h, DEPTH:, :] = jnp.broadcast_to(
+            keep * before_keep[d, :, lanes], (16, DEPTH)
+        ).astype(BF16)
+        scan_copy(k, d, h, sent, landed, p_send, p_recv).start()
+
+
+def scan_close(k, d, h, sent, landed, before, before_keep, p_send, p_recv):
+    _, _, source = partner(d, strides()[k])
 
     @pl.when(source)
     def _():
-        scan_copy(k, d, stride, sent, landed, p_send, p_recv).wait_recv()
-        for h in range(heads):
-            lanes = slice(h * DEPTH, (h + 1) * DEPTH)
-            keep = before_keep[d, :, lanes]
-            early = landed[k, d, h].astype(F32)
-            before[d, h] = keep * early[:DEPTH] + before[d, h]
-            before_keep[d, :, lanes] = keep * early[DEPTH : DEPTH + 1]
+        scan_copy(k, d, h, sent, landed, p_send, p_recv).wait_recv()
+        lanes = slice(h * DEPTH, (h + 1) * DEPTH)
+        keep = before_keep[d, :, lanes]
+        early = landed[k, d, h].astype(F32)
+        before[d, h] = keep * early[:DEPTH] + before[d, h]
+        before_keep[d, :, lanes] = keep * early[DEPTH : DEPTH + 1]
 
 
 def mixer_kernel(groups, *refs):
@@ -166,7 +162,7 @@
         held, gain, wide, gap, added, initial, head_gain, mix, pool_gain, wfull,
         acc, square, cols, rows_of, turned, query_pre, value, gated, ent, runs, inner, reach,
         starts, offsets, chunk_state, chunk_keep, state, offset, padded,
-        sent, landed, before, before_keep, given, taken, passed, brought, total,
+        sent, landed, before, before_keep, given, taken, passed, brought, total, kept_x, kept_scale,
         l_sem, s_sem, x_send, x_recv, f_send, f_recv, w_sem, b_sem, r_sem,
         rr_send, rr_recv, rl_send, rl_recv, p_send, p_recv, e_send, e_recv,
         a_send, a_recv, c_send, c_recv,
@@ -378,6 +374,16 @@
             reach[h, at, :DEPTH] = (q_f[:, lanes] * jnp.exp(a_col)).astype(BF16)
             reach[h, at, DEPTH:] = (q_b[:, lanes] * jnp.exp(b_col)).astype(BF16)
 
+    def project(j, x, scale, at):
+        return ((acc[j, at, :] + dot(x, wide[j, depth_of(far), :])) * scale).astype(BF16)
+
+    def late(c):
+        at, x, scale = piece(c), kept_x[...], kept_scale[...]
+        padded[pl.ds(pl.multiple_of(c * CHUNK + RIM, RIM), CHUNK), :] = project(5, x, scale, at)
+        query_pre[at, :] = project(0, x, scale, at)
+        gate = project(4, x, scale, at).astype(F32)
+        gated[at, :] = head_gain[...] / (1.0 + jnp.exp(-gate))
+
     def step(i, _):
         at = piece(i)
         crossing(i).wait_recv()
@@ -386,26 +392,19 @@
         @pl.when(i > 0)
         def _():
             ring_turn(i - 1)
+            late(i - 1)
             local(i - 1)
+
+        @pl.when(i == 1)
+        def _():
+            edge_start(1, length, padded, e_send, e_recv)
 
         relay(i).wait_recv()
         x, squares = normed(far, at)
         scale = lax.rsqrt((square[at, :] + squares) / features + EPSILON)
 
-        def project(j):
-            return ((acc[j, at, :] + dot(x, wide[j, depth_of(far), :])) * scale).astype(BF16)
-
-        pre_f, pre_b, values = project(1), project(2), project(3)
-        padded[pl.ds(pl.multiple_of(i * CHUNK + RIM, RIM), CHUNK), :] = project(5)
-
-        @pl.when(i == 0)
-        def _():
-            edge_start(1, length, padded, e_send, e_recv)
-
-        @pl.when(i == count - 1)
-        def _():
-            edge_start(0, length, padded, e_send, e_recv)
-
+        kept_x[...], kept_scale[...] = x, scale
+        pre_f, pre_b, values = (project(j, x, scale, at) for j in (1, 2, 3))
         value[at, :] = values
         enter_f, run_f = gates(pre_f.astype(F32), gap[0:1, :], lower_2)
         enter_b, run_b = gates(pre_b.astype(F32), gap[1:2, :], upper_2)
@@ -429,9 +428,6 @@
             chunk_state[i, h] = ends[:, DEPTH:]
             chunk_keep[i, :, lanes] = close_b[:, lanes] + b_end
             offset[0, :, lanes] = offset[0, :, lanes] + total_f
-        query_pre[at, :] = project(0)
-        gate = project(4).astype(F32)
-        gated[at, :] = head_gain[...] / (1.0 + jnp.exp(-gate))
         return 0
 
     lax.fori_loop(0, count, step, 0)
@@ -488,68 +484,67 @@
             ring_turn(e)
         w_relay.start()
 
+    def late_last():
+        late(count - 1)
+        edge_start(0, length, padded, e_send, e_recv)
+        local(count - 1)
+
+    def finished(c, h):
+        at, lanes = piece(c), slice(h * DEPTH, (h + 1) * DEPTH)
+        ages = jnp.exp(jnp.concatenate([offsets[0, c, :, lanes], offsets[1, c, :, lanes]], axis=1))
+        enter = (starts[c, h] + ages * turned[h]).astype(BF16)
+        both = inner[at, lanes] + dot_t(reach[h, at, :], enter)
+        both = both * lax.rsqrt(jnp.mean(both * both, axis=1, keepdims=True) + EPSILON)
+        given[h, at, :] = (both * gated[at, lanes]).astype(BF16)
+
+    def owner_of(k):
+        return jnp.where(k < 2, jnp.where(k == 0, across, opposite), jnp.where(k == 2, sibling, me))
+
+    def recur_copy(k, h):
+        there = owner_of(k)
+        at = pl.ds(pl.multiple_of(there * share, share), share)
+        return pltpu.make_async_remote_copy(
+            given.at[h, at], taken.at[me, h], c_send.at[h, k], c_recv.at[h, k],
+            device_id={"tp": there}, device_id_type=MESH,
+        )
+
+    def finish(h):
+        for d in range(2):
+            lanes = slice(d * DEPTH, (d + 1) * DEPTH)
+            keep = before_keep[d, :, h * DEPTH : (h + 1) * DEPTH]
+            turned[h, :, lanes] = keep * turned[h, :, lanes] + before[d, h]
+
+        def away(k, _):
+            for sub in range(subs):
+                finished(owner_of(k) * subs + sub, h)
+
+            @pl.when(k < 3)
+            def _():
+                recur_copy(k, h).start()
+
+            return 0
+
+        lax.fori_loop(0, 4, away, 0)
+
     scan = (sent, landed, before, before_keep, p_send, p_recv)
-    fillers = [
-        lambda: local(count - 1), pool_first, lambda: pool_away(1), ring_end,
-        lambda: pool_away(2), pool_home,
-    ]
-    if steps:
-        scan_start(0, 0, state, offset, *scan)
+    fillers = [late_last, pool_first, lambda: pool_away(1), ring_end, lambda: pool_away(2), pool_home]
     lax.fori_loop(0, count, descend, 0)
     for k in range(steps):
-        for d in range(2):
-            if k or d:
-                scan_start(k, d, state, offset, *scan)
+        for h in range(heads):
+            for d in range(2):
+                if k:
+                    scan_close(k - 1, d, h, *scan)
+                scan_start(k, d, h, state, offset, *scan)
         for filler in fillers[k * len(fillers) // steps : (k + 1) * len(fillers) // steps]:
             filler()
-        for d in range(2):
-            scan_close(k, d, state, *scan)
     if not steps:
         for filler in fillers:
             filler()
     for h in range(heads):
         for d in range(2):
-            lanes = slice(d * DEPTH, (d + 1) * DEPTH)
-            keep = before_keep[d, :, h * DEPTH : (h + 1) * DEPTH]
-            turned[h, :, lanes] = keep * turned[h, :, lanes] + before[d, h]
-
-    def finished(c):
-        at = piece(c)
-        for h in range(heads):
-            lanes = slice(h * DEPTH, (h + 1) * DEPTH)
-            ages = jnp.exp(
-                jnp.concatenate([offsets[0, c, :, lanes], offsets[1, c, :, lanes]], axis=1)
-            )
-            enter = (starts[c, h] + ages * turned[h]).astype(BF16)
-            both = inner[at, lanes] + dot_t(reach[h, at, :], enter)
-            both = both * lax.rsqrt(jnp.mean(both * both, axis=1, keepdims=True) + EPSILON)
-            yield lanes, (both * gated[at, lanes]).astype(BF16)
-
-    def recur_copy(t):
-        outward = t < 2 * subs
-        there = jnp.where(outward, jnp.where(lax.rem(t, 2) == 0, across, opposite), sibling)
-        sub = jnp.where(outward, t // 2, t - 2 * subs)
-        at = piece(there * subs + sub)
-        return there * subs + sub, pltpu.make_async_remote_copy(
-            given.at[at], taken.at[me, piece(sub)], c_send.at[t], c_recv.at[t],
-            device_id={"tp": there}, device_id_type=MESH,
-        )
-
-    def away(t, _):
-        c, copy = recur_copy(t)
-        for lanes, value_of in finished(c):
-            given[piece(c), lanes] = value_of
-        copy.start()
-        return 0
-
-    lax.fori_loop(0, 3 * subs, away, 0)
-
-    def home(s, _):
-        for lanes, value_of in finished(me * subs + s):
-            taken[me, piece(s), lanes] = value_of
-        return 0
-
-    lax.fori_loop(0, subs, home, 0)
+            if steps:
+                scan_close(steps - 1, d, h, *scan)
+        finish(h)
 
     tile = 512
     tiles = out.shape[1] // tile
@@ -557,28 +552,48 @@
     w_relay.wait_recv()
     for k in range(3):
         pool_copy(k).wait_recv()
-    for t in range(2 * subs, 3 * subs):
-        recur_copy(jnp.int32(t))[1].wait_recv()
-
-    def wide_part(j, _):
+    home = pl.ds(pl.multiple_of(me * share, share), share)
+
+    def wide_pool(j, _):
         lanes = pl.ds(pl.multiple_of(j * tile, tile), tile)
-        y = dot(taken[me], wfull[me, :depth, lanes])
-        y = y + dot(taken[sibling], wfull[sibling, :depth, lanes])
-        for r in range(4):
+        y = dot(brought[0], wfull[0, depth:, lanes])
+        for r in range(1, 4):
             y = y + dot(brought[r], wfull[r, depth:, lanes])
         total[:, lanes] = y
         return 0
 
+    lax.fori_loop(0, tiles, wide_pool, 0)
+    for h in range(heads):
+        recur_copy(2, h).wait_recv()
+        if h < heads - 1:
+            recur_copy(0, h).wait_recv()
+            recur_copy(1, h).wait_recv()
+
+    def wide_part(j, _):
+        lanes = pl.ds(pl.multiple_of(j * tile, tile), tile)
+        y = total[:, lanes]
+        here = jnp.concatenate([given[h, home, :] for h in range(heads)], axis=1)
+        y = y + dot(here, wfull[me, :depth, lanes])
+        here = jnp.concatenate([taken[sibling, h] for h in range(heads)], axis=1)
+        y = y + dot(here, wfull[sibling, :depth, lanes])
+        for h in range(heads - 1):
+            y = y + far_part(h, lanes)
+        total[:, lanes] = y
+        return 0
+
+    def far_part(h, lanes):
+        rows = slice(h * DEPTH, (h + 1) * DEPTH)
+        return dot(
+            jnp.concatenate([taken[across, h], taken[opposite, h]], axis=1),
+            jnp.concatenate([wfull[across, rows, lanes], wfull[opposite, rows, lanes]], axis=0),
+        )
+
     lax.fori_loop(0, tiles, wide_part, 0)
-    for s in range(subs):
-        recur_copy(jnp.int32(2 * s))[1].wait_recv()
-        recur_copy(jnp.int32(2 * s + 1))[1].wait_recv()
-        at = slice(s * CHUNK, (s + 1) * CHUNK)
-        for j in range(tiles):
-            lanes = slice(j * tile, (j + 1) * tile)
-            y = total[at, lanes] + dot(taken[across, at, :], wfull[across, :depth, lanes])
-            y = y + dot(taken[opposite, at, :], wfull[opposite, :depth, lanes])
-            out[at, lanes] = y.astype(BF16)
+    for k in range(2):
+        recur_copy(k, heads - 1).wait_recv()
+    for j in range(tiles):
+        lanes = slice(j * tile, (j + 1) * tile)
+        out[:, lanes] = (total[:, lanes] + far_part(heads - 1, lanes)).astype(BF16)
 
     w_across.wait_send()
     beside.wait_send()
@@ -608,12 +623,13 @@
 
             @pl.when(exists)
             def _():
-                scan_copy(k, d, strides()[k], sent, landed, p_send, p_recv).wait_send()
+                for h in range(heads):
+                    scan_copy(k, d, h, sent, landed, p_send, p_recv).wait_send()
 
     for k in range(3):
         pool_copy(k).wait_send()
-    for t in range(3 * subs):
-        recur_copy(jnp.int32(t))[1].wait_send()
+        for h in range(heads):
+            recur_copy(k, h).wait_send()
 
 
 def shards(
@@ -676,16 +692,18 @@
             pltpu.VMEM((steps, 2, heads, DEPTH + 16, DEPTH), BF16),
             pltpu.VMEM((2, heads, DEPTH, DEPTH), F32),
             pltpu.VMEM((2, 1, columns), F32),
-            pltpu.VMEM((length, columns), BF16),
-            pltpu.VMEM((4, share, columns), BF16),
+            pltpu.VMEM((heads, length, DEPTH), BF16),
+            pltpu.VMEM((4, heads, share, DEPTH), BF16),
             pltpu.VMEM((3, share, columns), BF16),
             pltpu.VMEM((4, share, columns), BF16),
             pltpu.VMEM((share, out_width), F32),
+            pltpu.VMEM((CHUNK, 2 * width), BF16),
+            pltpu.VMEM((CHUNK, 1), F32),
             dma((16,)), dma((2,)), dma((count,)), dma((count,)), dma((count,)), dma((count,)),
             dma((2,)), dma((2,)), dma((2,)),
             dma((rights,)), dma((rights,)), dma((lefts,)), dma((lefts,)),
-            dma((steps, 2)), dma((steps, 2)), dma((2,)), dma((2,)),
-            dma((3,)), dma((3,)), dma((3 * subs,)), dma((3 * subs,)),
+            dma((steps, 2, heads)), dma((steps, 2, heads)), dma((2,)), dma((2,)),
+            dma((3,)), dma((3,)), dma((heads, 3)), dma((heads, 3)),
         ],
         compiler_params=pltpu.CompilerParams(
             collective_id=0, has_side_effects=True, vmem_limit_bytes=VMEM_LIMIT

time: 61.7 us -> 60 us (0.972)
  Pallas kernels: 59.2 us -> 57.6 us
    pallas_call x1, Pallas kernels: 59.2 us -> 57.6 us  [shards(): pl.pallas_call(functools.partial(mixer_kernel, pool_mix.shape[0]), out_sh...]
where the time goes in v2:
time: 60 us; the launch traced here: 59.9 us
  Pallas kernels  57.6 us (96%)
  local copies, waits for them, and re-layouts  2.3 us (4%)
    pallas_call x1, Pallas kernels, shards(): pl.pallas_call(functools.partial(mixer_kernel, pool_mix.shape[0]), out_sh...  57.6 us
    unnamed x1, local copies, waits for them, and re-layouts  2.3 us

profile of v2, /device:TPU:1, one launch (start us, length us, event | category | flops | bytes accessed | tf_op | source)
XLA Modules:
  0.0 59.9 jit_solution(7888755359425108550)
XLA Ops:
  0.0 57.6 %mixer.1 = bf16[256,2048]{1,0:T(8,128)(2,1)} custom-call(bf16[1024,512]{1,0:T(8,128)(2,1)} %refs_0_.1, f32[1,2048]{1,0:T(1,128)} %bitcast.4, bf16[2048,256]{1,0:T(8,128)(2,1)} %refs_2_.1, bf16[2048,256]{1,0:T(8,128)(2,1)} %refs_3_.1, bf16[2048,256]{1,0:T(8,128)(2,1)} %refs_4_.1, bf16[2048,256]{1,0:T(8,128)(2,1)} %refs_5_.1, bf16[2048,256]{1,0:T(8,128)(2,1)} %refs_6_.1, ...), custom_call_target="tpu_custom_call" | custom-call | tf_op jit(solution)/shard_map/mixer/pallas_call | solution.py:660
  57.6 2.3 %copy.18 = bf16[256,2048]{1,0:T(8,128)(2,1)} copy(bf16[256,2048]{1,0:T(8,128)(2,1)} %mixer.1) | data formatting | bytes 2097152

commit v3 on v2

--- a/solution.py
+++ b/solution.py
@@ -15,7 +15,7 @@
 MESH = pl.DeviceIdType.MESH
 F32 = jnp.float32
 BF16 = jnp.bfloat16
-VMEM_LIMIT = 62 * 1024 * 1024
+VMEM_LIMIT = 52 * 1024 * 1024
 ANY = pl.BlockSpec(memory_space=pl.ANY)
 VM = pl.BlockSpec(memory_space=pltpu.VMEM)
 EXACT = lax.Precision.HIGHEST
@@ -110,13 +110,12 @@
         edge_copy(d, length, padded, e_send, e_recv).start()
 
 
-def edges_wait(length, padded, e_send, e_recv):
-    for d in range(2):
-        _, _, source = partner(d, 1)
-
-        @pl.when(source)
-        def _():
-            edge_copy(d, length, padded, e_send, e_recv).wait_recv()
+def edge_wait(d, length, padded, e_send, e_recv):
+    _, _, source = partner(d, 1)
+
+    @pl.when(source)
+    def _():
+        edge_copy(d, length, padded, e_send, e_recv).wait_recv()
 
 
 def scan_copy(k, d, h, sent, landed, p_send, p_recv):
@@ -164,7 +163,7 @@
         starts, offsets, chunk_state, chunk_keep, state, offset, padded,
         sent, landed, before, before_keep, given, taken, passed, brought, total, kept_x, kept_scale,
         l_sem, s_sem, x_send, x_recv, f_send, f_recv, w_sem, b_sem, r_sem,
-        rr_send, rr_recv, rl_send, rl_recv, p_send, p_recv, e_send, e_recv,
+        g_send, g_recv, q_send, q_recv, p_send, p_recv, e_send, e_recv,
         a_send, a_recv, c_send, c_recv,
     ) = refs[17:]
     me, sibling, across, opposite = peers()
@@ -201,7 +200,7 @@
     slab = 2 * depth // size
     half = slab // 2
     place, right, left = ring_place()
-    rights, lefts = 2 * (size // 2), 2 * (size - 1 - size // 2)
+    events = size - 1
 
     mine = pl.ds(pl.multiple_of(place * slab, slab), slab)
     w_across = pltpu.make_async_remote_copy(
@@ -212,43 +211,36 @@
         wfull.at[me], wfull.at[me], b_sem.at[0], b_sem.at[1],
         device_id={"tp": sibling}, device_id_type=MESH,
     )
-    w_relay = pltpu.make_async_remote_copy(
-        wfull.at[across], wfull.at[across], r_sem.at[0], r_sem.at[1],
-        device_id={"tp": sibling}, device_id_type=MESH,
-    )
-
-    def ring_right(e):
-        spot = lax.rem(place - e // 2 + size, size)
-        at = pl.ds(pl.multiple_of(spot * slab + lax.rem(e, 2) * half, half), half)
+    def w_pass(rows, send, recv):
         return pltpu.make_async_remote_copy(
-            wfull.at[across, at], wfull.at[across, at], rr_send.at[e], rr_recv.at[e],
-            device_id={"sp": right}, device_id_type=MESH,
-        )
-
-    def ring_left(e):
-        spot = lax.rem(place + e // 2, size)
-        at = pl.ds(pl.multiple_of(spot * slab + lax.rem(e, 2) * half, half), half)
+            wfull.at[across, rows], wfull.at[across, rows], send, recv,
+            device_id={"tp": sibling}, device_id_type=MESH,
+        )
+
+    def ring_rows(way, e):
+        spot = lax.rem(place + (e // 2 if way else size - e // 2), size)
+        side = 1 - lax.rem(e, 2) if way else lax.rem(e, 2)
+        return pl.ds(pl.multiple_of(spot * slab + side * half, half), half)
+
+    def ring_copy(way, e):
+        at = ring_rows(way, e)
         return pltpu.make_async_remote_copy(
-            wfull.at[across, at], wfull.at[across, at], rl_send.at[e], rl_recv.at[e],
-            device_id={"sp": left}, device_id_type=MESH,
-        )
+            wfull.at[across, at], wfull.at[across, at], g_send.at[way, e], g_recv.at[way, e],
+            device_id={"sp": left if way else right}, device_id_type=MESH,
+        )
+
+    def ring_relay(way, e):
+        return w_pass(ring_rows(way, e + 2), q_send.at[way, e], q_recv.at[way, e])
 
     def ring_turn(e):
-        @pl.when(e < rights)
-        def _():
-            ring_right(e).wait_recv()
-
-        @pl.when(e + 2 < rights)
-        def _():
-            ring_right(e + 2).start()
-
-        @pl.when(e < lefts)
-        def _():
-            ring_left(e).wait_recv()
-
-        @pl.when(e + 2 < lefts)
-        def _():
-            ring_left(e + 2).start()
+        for way in range(2):
+            ring_copy(way, e).wait_recv()
+
+            @pl.when(e + 2 < events)
+            def _():
+                ring_copy(way, e + 2).start()
+
+            ring_relay(way, e).start()
 
     beside = pltpu.make_async_remote_copy(
         held.at[me], held.at[me], s_sem.at[0], s_sem.at[1],
@@ -341,9 +333,10 @@
 
     lax.fori_loop(0, 4, own, 0)
     w_across.wait_recv()
-    for e in range(2):
-        ring_right(e).start()
-        ring_left(e).start()
+    for e in range(min(2, events)):
+        for way in range(2):
+            ring_copy(way, e).start()
+    w_pass(mine, r_sem.at[0], r_sem.at[1]).start()
 
     def gates(pre, gap_row, sums):
         enter = gap_row * (1.0 / (1.0 + jnp.exp(pre)))
@@ -391,9 +384,12 @@
 
         @pl.when(i > 0)
         def _():
-            ring_turn(i - 1)
             late(i - 1)
             local(i - 1)
+
+        @pl.when((i > 0) & (i <= events))
+        def _():
+            ring_turn(i - 1)
 
         @pl.when(i == 1)
         def _():
@@ -460,34 +456,60 @@
         here = padded[pl.ds(pl.multiple_of(begin + RIM, RIM), share), :].astype(F32)
         return (dot((mean - here).astype(BF16), mix[0]) * pool_gain[...]).astype(BF16)
 
-    others = (across, opposite, sibling)
-
-    def pool_copy(k):
+    def pool_copy(r, sender):
         return pltpu.make_async_remote_copy(
-            passed.at[k], brought.at[me], a_send.at[k], a_recv.at[k],
-            device_id={"tp": others[k]}, device_id_type=MESH,
-        )
-
-    def pool_away(k):
-        passed[k] = pooled(others[k])
-        pool_copy(k).start()
-
-    def pool_home():
-        brought[me] = pooled(me)
-
-    def pool_first():
-        edges_wait(length, padded, e_send, e_recv)
-        pool_away(0)
+            passed.at[r], brought.at[me], a_send.at[r], a_recv.at[sender],
+            device_id={"tp": jnp.int32(r)}, device_id_type=MESH,
+        )
+
+    def pool_away(r):
+        if r == 3:
+            edge_wait(1, length, padded, e_send, e_recv)
+        if r == 0:
+            edge_wait(0, length, padded, e_send, e_recv)
+        passed[r] = pooled(r)
+
+        @pl.when(me != r)
+        def _():
+            pool_copy(r, me).start()
 
     def ring_end():
-        for e in range(count - 1, max(rights, lefts)):
+        for e in range(count - 1, events):
             ring_turn(e)
-        w_relay.start()
 
     def late_last():
         late(count - 1)
         edge_start(0, length, padded, e_send, e_recv)
         local(count - 1)
+
+    tile = 512
+    tiles = out.shape[1] // tile
+
+    def wide_pool():
+        w_beside.wait_recv()
+        w_pass(mine, r_sem.at[0], r_sem.at[1]).wait_recv()
+
+        def landed_ring(e, _):
+            for way in range(2):
+                ring_relay(way, e).wait_recv()
+            return 0
+
+        lax.fori_loop(0, events, landed_ring, 0)
+        for r in range(4):
+            @pl.when(me != r)
+            def _():
+                pool_copy(r, r).wait_recv()
+
+        def part(j, _):
+            lanes = pl.ds(pl.multiple_of(j * tile, tile), tile)
+            y = 0.0
+            for r in range(4):
+                x = jnp.where(me == r, passed[r], brought[r])
+                y = y + dot(x, wfull[r, depth:, lanes])
+            total[:, lanes] = y
+            return 0
+
+        lax.fori_loop(0, tiles, part, 0)
 
     def finished(c, h):
         at, lanes = piece(c), slice(h * DEPTH, (h + 1) * DEPTH)
@@ -497,37 +519,31 @@
         both = both * lax.rsqrt(jnp.mean(both * both, axis=1, keepdims=True) + EPSILON)
         given[h, at, :] = (both * gated[at, lanes]).astype(BF16)
 
-    def owner_of(k):
-        return jnp.where(k < 2, jnp.where(k == 0, across, opposite), jnp.where(k == 2, sibling, me))
+    relations = (across, opposite, sibling, me)
 
     def recur_copy(k, h):
-        there = owner_of(k)
+        there = relations[k]
         at = pl.ds(pl.multiple_of(there * share, share), share)
         return pltpu.make_async_remote_copy(
             given.at[h, at], taken.at[me, h], c_send.at[h, k], c_recv.at[h, k],
             device_id={"tp": there}, device_id_type=MESH,
         )
 
-    def finish(h):
-        for d in range(2):
-            lanes = slice(d * DEPTH, (d + 1) * DEPTH)
-            keep = before_keep[d, :, h * DEPTH : (h + 1) * DEPTH]
-            turned[h, :, lanes] = keep * turned[h, :, lanes] + before[d, h]
-
-        def away(k, _):
-            for sub in range(subs):
-                finished(owner_of(k) * subs + sub, h)
-
-            @pl.when(k < 3)
-            def _():
-                recur_copy(k, h).start()
-
-            return 0
-
-        lax.fori_loop(0, 4, away, 0)
+    def away(k, h):
+        for sub in range(subs):
+            finished(relations[k] * subs + sub, h)
+        if k < 3:
+            recur_copy(k, h).start()
 
     scan = (sent, landed, before, before_keep, p_send, p_recv)
-    fillers = [late_last, pool_first, lambda: pool_away(1), ring_end, lambda: pool_away(2), pool_home]
+    fillers = [
+        (late_last, ring_end, lambda: pool_away(1), lambda: pool_away(2), lambda: pool_away(3)),
+        (lambda: pool_away(0),),
+        (wide_pool,),
+    ]
+    rounds = [[] for _ in range(max(steps, 1))]
+    for i, group in enumerate(fillers):
+        rounds[min(i, len(rounds) - 1)].extend(group)
     lax.fori_loop(0, count, descend, 0)
     for k in range(steps):
         for h in range(heads):
@@ -535,51 +551,26 @@
                 if k:
                     scan_close(k - 1, d, h, *scan)
                 scan_start(k, d, h, state, offset, *scan)
-        for filler in fillers[k * len(fillers) // steps : (k + 1) * len(fillers) // steps]:
+        for filler in rounds[k]:
             filler()
     if not steps:
-        for filler in fillers:
+        for filler in rounds[0]:
             filler()
     for h in range(heads):
         for d in range(2):
             if steps:
                 scan_close(steps - 1, d, h, *scan)
-        finish(h)
-
-    tile = 512
-    tiles = out.shape[1] // tile
-    w_beside.wait_recv()
-    w_relay.wait_recv()
-    for k in range(3):
-        pool_copy(k).wait_recv()
-    home = pl.ds(pl.multiple_of(me * share, share), share)
-
-    def wide_pool(j, _):
-        lanes = pl.ds(pl.multiple_of(j * tile, tile), tile)
-        y = dot(brought[0], wfull[0, depth:, lanes])
-        for r in range(1, 4):
-            y = y + dot(brought[r], wfull[r, depth:, lanes])
-        total[:, lanes] = y
-        return 0
-
-    lax.fori_loop(0, tiles, wide_pool, 0)
-    for h in range(heads):
-        recur_copy(2, h).wait_recv()
-        if h < heads - 1:
-            recur_copy(0, h).wait_recv()
-            recur_copy(1, h).wait_recv()
-
-    def wide_part(j, _):
-        lanes = pl.ds(pl.multiple_of(j * tile, tile), tile)
-        y = total[:, lanes]
-        here = jnp.concatenate([given[h, home, :] for h in range(heads)], axis=1)
-        y = y + dot(here, wfull[me, :depth, lanes])
-        here = jnp.concatenate([taken[sibling, h] for h in range(heads)], axis=1)
-        y = y + dot(here, wfull[sibling, :depth, lanes])
-        for h in range(heads - 1):
-            y = y + far_part(h, lanes)
-        total[:, lanes] = y
-        return 0
+            lanes = slice(d * DEPTH, (d + 1) * DEPTH)
+            keep = before_keep[d, :, h * DEPTH : (h + 1) * DEPTH]
+            turned[h, :, lanes] = keep * turned[h, :, lanes] + before[d, h]
+        for k in range(2):
+            away(k, h)
+    for k in (2, 3):
+        for h in range(heads):
+            away(k, h)
+
+    def all_heads(rows):
+        return jnp.concatenate([rows(h) for h in range(heads)], axis=1)
 
     def far_part(h, lanes):
         rows = slice(h * DEPTH, (h + 1) * DEPTH)
@@ -588,17 +579,32 @@
             jnp.concatenate([wfull[across, rows, lanes], wfull[opposite, rows, lanes]], axis=0),
         )
 
-    lax.fori_loop(0, tiles, wide_part, 0)
-    for k in range(2):
-        recur_copy(k, heads - 1).wait_recv()
+    for h in range(heads):
+        recur_copy(2, h).wait_recv()
+    home = pl.ds(pl.multiple_of(me * share, share), share)
     for j in range(tiles):
         lanes = slice(j * tile, (j + 1) * tile)
-        out[:, lanes] = (total[:, lanes] + far_part(heads - 1, lanes)).astype(BF16)
+        y = total[:, lanes] + dot(
+            all_heads(lambda h: given[h, home, :]), wfull[me, :depth, lanes]
+        )
+        total[:, lanes] = y + dot(
+            all_heads(lambda h: taken[sibling, h]), wfull[sibling, :depth, lanes]
+        )
+    for h in range(heads):
+        for k in range(2):
+            recur_copy(k, h).wait_recv()
+        for j in range(tiles):
+            lanes = slice(j * tile, (j + 1) * tile)
+            y = total[:, lanes] + far_part(h, lanes)
+            if h == heads - 1:
+                out[:, lanes] = y.astype(BF16)
+            else:
+                total[:, lanes] = y
 
     w_across.wait_send()
     beside.wait_send()
     w_beside.wait_send()
-    w_relay.wait_send()
+    w_pass(mine, r_sem.at[0], r_sem.at[1]).wait_send()
 
     def sent_pieces(i, _):
         crossing(i).wait_send()
@@ -606,10 +612,14 @@
         return 0
 
     lax.fori_loop(0, count, sent_pieces, 0)
-    for e in range(rights):
-        ring_right(e).wait_send()
-    for e in range(lefts):
-        ring_left(e).wait_send()
+
+    def sent_ring(e, _):
+        for way in range(2):
+            ring_copy(way, e).wait_send()
+            ring_relay(way, e).wait_send()
+        return 0
+
+    lax.fori_loop(0, events, sent_ring, 0)
     for d in range(2):
         exists, _, _ = partner(d, 1)
 
@@ -626,9 +636,13 @@
                 for h in range(heads):
                     scan_copy(k, d, h, sent, landed, p_send, p_recv).wait_send()
 
-    for k in range(3):
-        pool_copy(k).wait_send()
-        for h in range(heads):
+    for r in range(4):
+        @pl.when(me != r)
+        def _():
+            pool_copy(r, me).wait_send()
+
+    for h in range(heads):
+        for k in range(3):
             recur_copy(k, h).wait_send()
 
 
@@ -647,7 +661,7 @@
     depth, out_width = w_out_recur.shape
     steps = len(strides())
     size = ring_size()
-    rights, lefts = 2 * (size // 2), 2 * (size - 1 - size // 2)
+    events = size - 1
     dma = pltpu.SemaphoreType.DMA
     operands = (
         tokens, norm_gain[None, :], *weights, forget_gap, added_log_retention.T, initial_state,
@@ -659,7 +673,7 @@
 
     return pl.pallas_call(
         functools.partial(mixer_kernel, pool_mix.shape[0]),
-        out_shape=jax.ShapeDtypeStruct((share, out_width), BF16),
+        out_shape=pltpu.VMEM((share, out_width), BF16),
         in_specs=[ANY] * len(operands),
         out_specs=VM,
         scratch_shapes=[
@@ -694,22 +708,22 @@
             pltpu.VMEM((2, 1, columns), F32),
             pltpu.VMEM((heads, length, DEPTH), BF16),
             pltpu.VMEM((4, heads, share, DEPTH), BF16),
-            pltpu.VMEM((3, share, columns), BF16),
+            pltpu.VMEM((4, share, columns), BF16),
             pltpu.VMEM((4, share, columns), BF16),
             pltpu.VMEM((share, out_width), F32),
             pltpu.VMEM((CHUNK, 2 * width), BF16),
             pltpu.VMEM((CHUNK, 1), F32),
             dma((16,)), dma((2,)), dma((count,)), dma((count,)), dma((count,)), dma((count,)),
             dma((2,)), dma((2,)), dma((2,)),
-            dma((rights,)), dma((rights,)), dma((lefts,)), dma((lefts,)),
+            dma((2, events)), dma((2, events)), dma((2, events)), dma((2, events)),
             dma((steps, 2, heads)), dma((steps, 2, heads)), dma((2,)), dma((2,)),
-            dma((3,)), dma((3,)), dma((heads, 3)), dma((heads, 3)),
+            dma((4,)), dma((4,)), dma((heads, 3)), dma((heads, 3)),
         ],
         compiler_params=pltpu.CompilerParams(
             collective_id=0, has_side_effects=True, vmem_limit_bytes=VMEM_LIMIT
         ),
         name="mixer",
-    )(*operands)
+    )(*(pltpu.with_memory_space_constraint(x, pltpu.HBM) for x in operands))
 
 
 def solution(mesh):

time: 60 us -> 58.3 us (0.972)
  local copies, waits for them, and re-layouts: 2.3 us -> 0.97 us
    unnamed x1, local copies, waits for them, and re-layouts: 2.3 us -> 0.97 us
where the time goes in v3:
time: 58.3 us; the launch traced here: 58.2 us
  Pallas kernels  57.2 us (98%)
  local copies, waits for them, and re-layouts  0.97 us (2%)
    pallas_call x1, Pallas kernels, shards(): pl.pallas_call(functools.partial(mixer_kernel, pool_mix.shape[0]), out_sh...  57.2 us

profile of v3, /device:TPU:1, one launch (start us, length us, event | category | flops | bytes accessed | tf_op | source)
XLA Modules:
  0.0 58.2 jit_solution(4863543189358423938)
XLA Ops:
  0.0 57.2 %mixer.1 = bf16[256,2048]{1,0:T(8,128)(2,1)S(1)} custom-call(bf16[1024,512]{1,0:T(8,128)(2,1)} %refs_0_.1, f32[1,2048]{1,0:T(1,128)} %bitcast.4, bf16[2048,256]{1,0:T(8,128)(2,1)} %refs_2_.1, bf16[2048,256]{1,0:T(8,128)(2,1)} %refs_3_.1, bf16[2048,256]{1,0:T(8,128)(2,1)} %refs_4_.1, bf16[2048,256]{1,0:T(8,128)(2,1)} %refs_5_.1, bf16[2048,256]{1,0:T(8,128)(2,1)} %refs_6_.1, ...), custom_call_target="tpu_custom_call" | custom-call | tf_op jit(solution)/shard_map/mixer/pallas_call | solution.py:674
  57.2 1.0 %copy.18 = bf16[256,2048]{1,0:T(8,128)(2,1)} copy(bf16[256,2048]{1,0:T(8,128)(2,1)S(1)} %mixer.1) | data formatting | bytes 2097152

commit v4 on v3

--- a/solution.py
+++ b/solution.py
@@ -50,7 +50,11 @@
 def partner(d, stride):
     me, count = lax.axis_index("sp"), lax.axis_size("sp")
     above, below = me + stride < count, me >= stride
-    return (above, me + stride, below) if d == 0 else (below, me - stride, above)
+    if isinstance(d, int):
+        return (above, me + stride, below) if d == 0 else (below, me - stride, above)
+    target = jnp.where(d == 0, me + stride, me - stride)
+    source = jnp.where(d == 0, me - stride, me + stride)
+    return (target >= 0) & (target < count), target, (source >= 0) & (source < count)
 
 
 def ring_size():
@@ -95,10 +99,10 @@
 
 def edge_copy(d, length, padded, e_send, e_recv):
     _, target, _ = partner(d, 1)
-    begin, there = (length, 0) if d == 0 else (RIM, RIM + length)
+    there = 0 if d == 0 else RIM + length
     return pltpu.make_async_remote_copy(
-        padded.at[pl.ds(begin, RIM)], padded.at[pl.ds(there, RIM)], e_send.at[d], e_recv.at[d],
-        device_id={"sp": target}, device_id_type=MESH,
+        padded.at[pl.ds(length if d == 0 else RIM, RIM)], padded.at[pl.ds(there, RIM)],
+        e_send.at[d], e_recv.at[d], device_id={"sp": target}, device_id_type=MESH,
     )
 
 
@@ -121,7 +125,7 @@
 def scan_copy(k, d, h, sent, landed, p_send, p_recv):
     _, target, _ = partner(d, strides()[k])
     return pltpu.make_async_remote_copy(
-        sent.at[k, d, h], landed.at[k, d, h], p_send.at[k, d, h], p_recv.at[k, d, h],
+        sent.at[k, d, h], landed.at[k, d, h], p_send.at[k, d], p_recv.at[k, d, h],
         device_id={"sp": target}, device_id_type=MESH,
     )
 
@@ -162,9 +166,8 @@
         acc, square, cols, rows_of, turned, query_pre, value, gated, ent, runs, inner, reach,
         starts, offsets, chunk_state, chunk_keep, state, offset, padded,
         sent, landed, before, before_keep, given, taken, passed, brought, total, kept_x, kept_scale,
-        l_sem, s_sem, x_send, x_recv, f_send, f_recv, w_sem, b_sem, r_sem,
-        g_send, g_recv, q_send, q_recv, p_send, p_recv, e_send, e_recv,
-        a_send, a_recv, c_send, c_recv,
+        l_sem, t_send, w_send, s_recv, x_recv, f_recv, w_recv, q_recv, g_recv,
+        p_send, p_recv, e_send, e_recv, a_send, a_recv, c_send, c_recv,
     ) = refs[17:]
     me, sibling, across, opposite = peers()
     length, width = held.shape[1:]
@@ -179,9 +182,9 @@
 
     own_w = [
         pltpu.make_async_copy(h_recur, wfull.at[me, pl.ds(0, depth)], l_sem.at[0]),
-        pltpu.make_async_copy(h_pool, wfull.at[me, pl.ds(depth, depth)], l_sem.at[1]),
+        pltpu.make_async_copy(h_pool, wfull.at[me, pl.ds(depth, depth)], l_sem.at[0]),
     ]
-    own_t = pltpu.make_async_copy(h_tokens, held.at[me], l_sem.at[2])
+    own_t = pltpu.make_async_copy(h_tokens, held.at[me], l_sem.at[1])
     small = [
         pltpu.make_async_copy(a, b, l_sem.at[3 + i])
         for i, (a, b) in enumerate((
@@ -190,7 +193,7 @@
         ))
     ]
     loads = [
-        pltpu.make_async_copy(w, wide.at[i], l_sem.at[10 + i]) for i, w in enumerate(h_weights)
+        pltpu.make_async_copy(w, wide.at[i], l_sem.at[2]) for i, w in enumerate(h_weights)
     ]
     for copy in own_w + [own_t] + small + loads:
         copy.start()
@@ -204,16 +207,16 @@
 
     mine = pl.ds(pl.multiple_of(place * slab, slab), slab)
     w_across = pltpu.make_async_remote_copy(
-        wfull.at[me, mine], wfull.at[me, mine], w_sem.at[0], w_sem.at[1],
+        wfull.at[me, mine], wfull.at[me, mine], w_send.at[0], w_recv.at[0],
         device_id={"tp": across}, device_id_type=MESH,
     )
     w_beside = pltpu.make_async_remote_copy(
-        wfull.at[me], wfull.at[me], b_sem.at[0], b_sem.at[1],
+        wfull.at[me], wfull.at[me], w_send.at[0], q_recv.at[0],
         device_id={"tp": sibling}, device_id_type=MESH,
     )
-    def w_pass(rows, send, recv):
+    def w_pass(rows):
         return pltpu.make_async_remote_copy(
-            wfull.at[across, rows], wfull.at[across, rows], send, recv,
+            wfull.at[across, rows], wfull.at[across, rows], w_send.at[0], q_recv.at[0],
             device_id={"tp": sibling}, device_id_type=MESH,
         )
 
@@ -225,25 +228,25 @@
     def ring_copy(way, e):
         at = ring_rows(way, e)
         return pltpu.make_async_remote_copy(
-            wfull.at[across, at], wfull.at[across, at], g_send.at[way, e], g_recv.at[way, e],
+            wfull.at[across, at], wfull.at[across, at], w_send.at[0], g_recv.at[e],
             device_id={"sp": left if way else right}, device_id_type=MESH,
         )
 
-    def ring_relay(way, e):
-        return w_pass(ring_rows(way, e + 2), q_send.at[way, e], q_recv.at[way, e])
-
     def ring_turn(e):
+        landed_slab = wfull.at[across, pl.ds(0, slab)]
+        pltpu.make_async_remote_copy(
+            landed_slab, landed_slab, w_send.at[0], g_recv.at[e],
+            device_id={"sp": right}, device_id_type=MESH,
+        ).wait_recv()
         for way in range(2):
-            ring_copy(way, e).wait_recv()
-
             @pl.when(e + 2 < events)
             def _():
                 ring_copy(way, e + 2).start()
 
-            ring_relay(way, e).start()
+            w_pass(ring_rows(way, e + 2)).start()
 
     beside = pltpu.make_async_remote_copy(
-        held.at[me], held.at[me], s_sem.at[0], s_sem.at[1],
+        held.at[me], held.at[me], t_send.at[0], s_recv.at[0],
         device_id={"tp": sibling}, device_id_type=MESH,
     )
 
@@ -252,18 +255,17 @@
 
     def crossing(i):
         return pltpu.make_async_remote_copy(
-            held.at[me, piece(i)], held.at[me, piece(i)], x_send.at[i], x_recv.at[i],
+            held.at[me, piece(i)], held.at[me, piece(i)], t_send.at[0], x_recv.at[i],
             device_id={"tp": across}, device_id_type=MESH,
         )
 
     def relay(i):
         return pltpu.make_async_remote_copy(
-            held.at[across, piece(i)], held.at[across, piece(i)], f_send.at[i], f_recv.at[i],
+            held.at[across, piece(i)], held.at[across, piece(i)], t_send.at[0], f_recv.at[i],
             device_id={"tp": sibling}, device_id_type=MESH,
         )
 
-    for copy in own_w:
-        copy.wait()
+    pltpu.make_async_copy(wfull.at[across], wfull.at[me], l_sem.at[0]).wait()
     w_across.start()
     own_t.wait()
     beside.start()
@@ -319,8 +321,7 @@
     def depth_of(first):
         return pl.ds(pl.multiple_of(first * width, 2 * width), 2 * width)
 
-    for copy in loads:
-        copy.wait()
+    pltpu.make_async_copy(wide, wide, l_sem.at[2]).wait()
     beside.wait_recv()
 
     def own(i, _):
@@ -336,7 +337,7 @@
     for e in range(min(2, events)):
         for way in range(2):
             ring_copy(way, e).start()
-    w_pass(mine, r_sem.at[0], r_sem.at[1]).start()
+    w_pass(mine).start()
 
     def gates(pre, gap_row, sums):
         enter = gap_row * (1.0 / (1.0 + jnp.exp(pre)))
@@ -370,9 +371,12 @@
     def project(j, x, scale, at):
         return ((acc[j, at, :] + dot(x, wide[j, depth_of(far), :])) * scale).astype(BF16)
 
+    def late_pool(c):
+        rows = project(5, kept_x[...], kept_scale[...], piece(c))
+        padded[pl.ds(pl.multiple_of(c * CHUNK + RIM, RIM), CHUNK), :] = rows
+
     def late(c):
         at, x, scale = piece(c), kept_x[...], kept_scale[...]
-        padded[pl.ds(pl.multiple_of(c * CHUNK + RIM, RIM), CHUNK), :] = project(5, x, scale, at)
         query_pre[at, :] = project(0, x, scale, at)
         gate = project(4, x, scale, at).astype(F32)
         gated[at, :] = head_gain[...] / (1.0 + jnp.exp(-gate))
@@ -384,6 +388,7 @@
 
         @pl.when(i > 0)
         def _():
+            late_pool(i - 1)
             late(i - 1)
             local(i - 1)
 
@@ -456,60 +461,87 @@
         here = padded[pl.ds(pl.multiple_of(begin + RIM, RIM), share), :].astype(F32)
         return (dot((mean - here).astype(BF16), mix[0]) * pool_gain[...]).astype(BF16)
 
-    def pool_copy(r, sender):
+    def pool_copy(r):
         return pltpu.make_async_remote_copy(
-            passed.at[r], brought.at[me], a_send.at[r], a_recv.at[sender],
+            passed.at[r], brought.at[me], a_send.at[0], a_recv.at[0],
             device_id={"tp": jnp.int32(r)}, device_id_type=MESH,
         )
+
+    pool_all = pltpu.make_async_remote_copy(
+        passed.at[pl.ds(0, 3)], brought.at[pl.ds(0, 3)], a_send.at[0], a_recv.at[0],
+        device_id={"tp": sibling}, device_id_type=MESH,
+    )
 
     def pool_away(r):
         if r == 3:
             edge_wait(1, length, padded, e_send, e_recv)
         if r == 0:
             edge_wait(0, length, padded, e_send, e_recv)
-        passed[r] = pooled(r)
+        rows = pooled(r)
+        passed[r] = rows
+
+        @pl.when(me == r)
+        def _():
+            brought[r] = rows
 
         @pl.when(me != r)
         def _():
-            pool_copy(r, me).start()
+            pool_copy(r).start()
 
     def ring_end():
         for e in range(count - 1, events):
             ring_turn(e)
 
+    def drain_gather():
+        for block, sem in ((held, t_send), (wfull, w_send)):
+            rows = block.at[pl.ds(0, 3)]
+            pltpu.make_async_remote_copy(
+                rows, rows, sem.at[0], s_recv.at[0],
+                device_id={"tp": sibling}, device_id_type=MESH,
+            ).wait_send()
+
+    def drain_scan():
+        for d in range(2):
+            exists, _, _ = partner(d, 1)
+
+            @pl.when(exists)
+            def _():
+                edge_copy(d, length, padded, e_send, e_recv).wait_send()
+
+        for k in range(steps):
+            for d in range(2):
+                exists, _, _ = partner(d, strides()[k])
+
+                @pl.when(exists)
+                def _():
+                    pltpu.make_async_remote_copy(
+                        sent.at[k, d], sent.at[k, d], p_send.at[k, d], p_recv.at[k, d, 0],
+                        device_id={"tp": sibling}, device_id_type=MESH,
+                    ).wait_send()
+
+        pool_all.wait_send()
+
     def late_last():
+        late_pool(count - 1)
+        edge_start(0, length, padded, e_send, e_recv)
         late(count - 1)
-        edge_start(0, length, padded, e_send, e_recv)
         local(count - 1)
 
     tile = 512
     tiles = out.shape[1] // tile
 
     def wide_pool():
-        w_beside.wait_recv()
-        w_pass(mine, r_sem.at[0], r_sem.at[1]).wait_recv()
-
-        def landed_ring(e, _):
-            for way in range(2):
-                ring_relay(way, e).wait_recv()
-            return 0
-
-        lax.fori_loop(0, events, landed_ring, 0)
-        for r in range(4):
-            @pl.when(me != r)
-            def _():
-                pool_copy(r, r).wait_recv()
-
-        def part(j, _):
-            lanes = pl.ds(pl.multiple_of(j * tile, tile), tile)
-            y = 0.0
-            for r in range(4):
-                x = jnp.where(me == r, passed[r], brought[r])
-                y = y + dot(x, wfull[r, depth:, lanes])
+        pltpu.make_async_remote_copy(
+            wfull.at[pl.ds(0, 2)], wfull.at[pl.ds(0, 2)], w_send.at[0], q_recv.at[0],
+            device_id={"tp": sibling}, device_id_type=MESH,
+        ).wait_recv()
+        pool_all.wait_recv()
+        for j in range(tiles):
+            lanes = slice(j * tile, (j + 1) * tile)
+            y = dot(brought[0], wfull[0, depth:, lanes])
+            for r in range(1, 4):
+                y = y + dot(brought[r], wfull[r, depth:, lanes])
             total[:, lanes] = y
-            return 0
-
-        lax.fori_loop(0, tiles, part, 0)
 
     def finished(c, h):
         at, lanes = piece(c), slice(h * DEPTH, (h + 1) * DEPTH)
@@ -525,8 +557,15 @@
         there = relations[k]
         at = pl.ds(pl.multiple_of(there * share, share), share)
         return pltpu.make_async_remote_copy(
-            given.at[h, at], taken.at[me, h], c_send.at[h, k], c_recv.at[h, k],
+            given.at[h, at], taken.at[me, h], c_send.at[0], c_recv.at[heads if k == 2 else h],
             device_id={"tp": there}, device_id_type=MESH,
+        )
+
+    def recur_wait(owners, count, h):
+        rows = taken.at[pl.ds(0, owners), pl.ds(0, count)]
+        return pltpu.make_async_remote_copy(
+            rows, rows, c_send.at[0], c_recv.at[h],
+            device_id={"tp": sibling}, device_id_type=MESH,
         )
 
     def away(k, h):
@@ -537,23 +576,29 @@
 
     scan = (sent, landed, before, before_keep, p_send, p_recv)
     fillers = [
-        (late_last, ring_end, lambda: pool_away(1), lambda: pool_away(2), lambda: pool_away(3)),
-        (lambda: pool_away(0),),
-        (wide_pool,),
+        [late_last, ring_end] + [functools.partial(pool_away, r) for r in (1, 2, 3)],
+        [lambda: pool_away(0), drain_gather],
+        [wide_pool],
     ]
+    first = 1 - lax.rem(lax.axis_index("sp"), 2)
     rounds = [[] for _ in range(max(steps, 1))]
     for i, group in enumerate(fillers):
         rounds[min(i, len(rounds) - 1)].extend(group)
-    lax.fori_loop(0, count, descend, 0)
     for k in range(steps):
-        for h in range(heads):
-            for d in range(2):
-                if k:
-                    scan_close(k - 1, d, h, *scan)
+        if k == 0:
+            for h in range(heads):
+                scan_start(0, 0, h, state, offset, *scan)
+            lax.fori_loop(0, count, descend, 0)
+            for h in range(heads):
+                scan_start(0, 1, h, state, offset, *scan)
+        for h in range(heads if k else 0):
+            for d in (first, 1 - first):
+                scan_close(k - 1, d, h, *scan)
                 scan_start(k, d, h, state, offset, *scan)
         for filler in rounds[k]:
             filler()
     if not steps:
+        lax.fori_loop(0, count, descend, 0)
         for filler in rounds[0]:
             filler()
     for h in range(heads):
@@ -579,8 +624,7 @@
             jnp.concatenate([wfull[across, rows, lanes], wfull[opposite, rows, lanes]], axis=0),
         )
 
-    for h in range(heads):
-        recur_copy(2, h).wait_recv()
+    recur_wait(1, heads, heads).wait_recv()
     home = pl.ds(pl.multiple_of(me * share, share), share)
     for j in range(tiles):
         lanes = slice(j * tile, (j + 1) * tile)
@@ -590,9 +634,9 @@
         total[:, lanes] = y + dot(
             all_heads(lambda h: taken[sibling, h]), wfull[sibling, :depth, lanes]
         )
+    drain_scan()
     for h in range(heads):
-        for k in range(2):
-            recur_copy(k, h).wait_recv()
+        recur_wait(1, 2, h).wait_recv()
         for j in range(tiles):
             lanes = slice(j * tile, (j + 1) * tile)
             y = total[:, lanes] + far_part(h, lanes)
@@ -601,49 +645,7 @@
             else:
                 total[:, lanes] = y
 
-    w_across.wait_send()
-    beside.wait_send()
-    w_beside.wait_send()
-    w_pass(mine, r_sem.at[0], r_sem.at[1]).wait_send()
-
-    def sent_pieces(i, _):
-        crossing(i).wait_send()
-        relay(i).wait_send()
-        return 0
-
-    lax.fori_loop(0, count, sent_pieces, 0)
-
-    def sent_ring(e, _):
-        for way in range(2):
-            ring_copy(way, e).wait_send()
-            ring_relay(way, e).wait_send()
-        return 0
-
-    lax.fori_loop(0, events, sent_ring, 0)
-    for d in range(2):
-        exists, _, _ = partner(d, 1)
-
-        @pl.when(exists)
-        def _():
-            edge_copy(d, length, padded, e_send, e_recv).wait_send()
-
-    for k in range(steps):
-        for d in range(2):
-            exists, _, _ = partner(d, strides()[k])
-
-            @pl.when(exists)
-            def _():
-                for h in range(heads):
-                    scan_copy(k, d, h, sent, landed, p_send, p_recv).wait_send()
-
-    for r in range(4):
-        @pl.when(me != r)
-        def _():
-            pool_copy(r, me).wait_send()
-
-    for h in range(heads):
-        for k in range(3):
-            recur_copy(k, h).wait_send()
+    recur_wait(3, heads, 0).wait_send()
 
 
 def shards(
@@ -713,11 +715,10 @@
             pltpu.VMEM((share, out_width), F32),
             pltpu.VMEM((CHUNK, 2 * width), BF16),
             pltpu.VMEM((CHUNK, 1), F32),
-            dma((16,)), dma((2,)), dma((count,)), dma((count,)), dma((count,)), dma((count,)),
-            dma((2,)), dma((2,)), dma((2,)),
-            dma((2, events)), dma((2, events)), dma((2, events)), dma((2, events)),
-            dma((steps, 2, heads)), dma((steps, 2, heads)), dma((2,)), dma((2,)),
-            dma((4,)), dma((4,)), dma((heads, 3)), dma((heads, 3)),
+            dma((10,)), dma((1,)), dma((1,)), dma((1,)), dma((count,)), dma((count,)),
+            dma((1,)), dma((1,)), dma((events,)),
+            dma((steps, 2)), dma((steps, 2, heads)), dma((2,)), dma((2,)),
+            dma((1,)), dma((1,)), dma((1,)), dma((heads + 1,)),
         ],
         compiler_params=pltpu.CompilerParams(
             collective_id=0, has_side_effects=True, vmem_limit_bytes=VMEM_LIMIT

time: 58.3 us -> 57.1 us (0.979)
  Pallas kernels: 57.2 us -> 56 us
    pallas_call x1, Pallas kernels: 57.2 us -> 56 us  [shards(): pl.pallas_call(functools.partial(mixer_kernel, pool_mix.shape[0]), out_sh...]
where the time goes in v4:
time: 57.1 us; the launch traced here: 56.9 us
  Pallas kernels  56 us (98%)
  local copies, waits for them, and re-layouts  0.97 us (2%)
    pallas_call x1, Pallas kernels, shards(): pl.pallas_call(functools.partial(mixer_kernel, pool_mix.shape[0]), out_sh...  56 us

profile of v4, /device:TPU:1, one launch (start us, length us, event | category | flops | bytes accessed | tf_op | source)
XLA Modules:
  0.0 56.9 jit_solution(15450572558744417294)
XLA Ops:
  0.0 56.0 %mixer.1 = bf16[256,2048]{1,0:T(8,128)(2,1)S(1)} custom-call(bf16[1024,512]{1,0:T(8,128)(2,1)} %refs_0_.1, f32[1,2048]{1,0:T(1,128)} %bitcast.4, bf16[2048,256]{1,0:T(8,128)(2,1)} %refs_2_.1, bf16[2048,256]{1,0:T(8,128)(2,1)} %refs_3_.1, bf16[2048,256]{1,0:T(8,128)(2,1)} %refs_4_.1, bf16[2048,256]{1,0:T(8,128)(2,1)} %refs_5_.1, bf16[2048,256]{1,0:T(8,128)(2,1)} %refs_6_.1, ...), custom_call_target="tpu_custom_call" | custom-call | tf_op jit(solution)/shard_map/mixer/pallas_call | solution.py:676
  56.0 1.0 %copy.18 = bf16[256,2048]{1,0:T(8,128)(2,1)} copy(bf16[256,2048]{1,0:T(8,128)(2,1)S(1)} %mixer.1) | data formatting | bytes 2097152

commit v5 on v4

--- a/solution.py
+++ b/solution.py
@@ -12,6 +12,7 @@
 EPSILON = 1e-06
 RIM = 16
 RING = 8
+GROUP = 4
 MESH = pl.DeviceIdType.MESH
 F32 = jnp.float32
 BF16 = jnp.bfloat16
@@ -42,19 +43,39 @@
     return me, sibling, across, lax.rem(sibling + 2, 4)
 
 
-def strides():
-    count = lax.axis_size("sp")
-    return [1 << k for k in range(count.bit_length()) if 1 << k < count]
-
-
 def partner(d, stride):
     me, count = lax.axis_index("sp"), lax.axis_size("sp")
     above, below = me + stride < count, me >= stride
-    if isinstance(d, int):
-        return (above, me + stride, below) if d == 0 else (below, me - stride, above)
-    target = jnp.where(d == 0, me + stride, me - stride)
-    source = jnp.where(d == 0, me - stride, me + stride)
-    return (target >= 0) & (target < count), target, (source >= 0) & (source < count)
+    return (above, me + stride, below) if d == 0 else (below, me - stride, above)
+
+
+def group_size():
+    return min(GROUP, lax.axis_size("sp"))
+
+
+def group_strides():
+    count = lax.axis_size("sp") // group_size()
+    return [1 << k for k in range(count.bit_length()) if 1 << k < count]
+
+
+def group_place():
+    me = lax.axis_index("sp")
+    return me // group_size(), lax.rem(me, group_size())
+
+
+def raw_partner(d, j):
+    (_, place), me, size = group_place(), lax.axis_index("sp"), group_size()
+    above, below = place + j < size, place >= j
+    return (above, me + j, below) if d == 0 else (below, me - j, above)
+
+
+def group_partner(d, stride):
+    (group, place), size = group_place(), group_size()
+    count = lax.axis_size("sp") // size
+    above, below = group + stride < count, group >= stride
+    if d == 0:
+        return above & (place == size - 1), group + stride, below
+    return below & (place == 0), group - stride, above
 
 
 def ring_size():
@@ -82,18 +103,23 @@
         pl.semaphore_signal(barrier, inc=1, device_id={"tp": device}, device_id_type=MESH)
     for device in (right, left):
         pl.semaphore_signal(barrier, inc=1, device_id={"sp": device}, device_id_type=MESH)
-    number = jnp.int32(5)
-    for stride in strides():
+    size, (group, place) = group_size(), group_place()
+    for j in range(1, size):
+        target = group * size + lax.rem(place + j, size)
+        pl.semaphore_signal(barrier, inc=1, device_id={"sp": target}, device_id_type=MESH)
+    number = jnp.int32(5 + size - 1)
+    for stride in group_strides():
         for d in range(2):
-            exists, target, _ = partner(d, stride)
-
-            @pl.when(exists)
+            sends, _, gets = group_partner(d, stride)
+            source = (group - stride) * size + size - 1 if d == 0 else (group + stride) * size
+
+            @pl.when(gets)
             def _():
                 pl.semaphore_signal(
-                    barrier, inc=1, device_id={"sp": target}, device_id_type=MESH
+                    barrier, inc=1, device_id={"sp": source}, device_id_type=MESH
                 )
 
-            number = number + jnp.where(exists, 1, 0)
+            number = number + jnp.where(sends, size, 0)
     pl.semaphore_wait(barrier, number)
 
 
@@ -122,18 +148,21 @@
         edge_copy(d, length, padded, e_send, e_recv).wait_recv()
 
 
-def scan_copy(k, d, h, sent, landed, p_send, p_recv):
-    _, target, _ = partner(d, strides()[k])
+def scan_copy(slot, k, d, h, target, sent, landed, p_send, p_recv):
     return pltpu.make_async_remote_copy(
-        sent.at[k, d, h], landed.at[k, d, h], p_send.at[k, d], p_recv.at[k, d, h],
+        sent.at[k, d, h], landed.at[slot, d, h], p_send.at[slot, d], p_recv.at[slot, d, h],
         device_id={"sp": target}, device_id_type=MESH,
     )
 
 
 def scan_start(k, d, h, state, offset, sent, landed, before, before_keep, p_send, p_recv):
-    exists, _, _ = partner(d, strides()[k])
-
-    @pl.when(exists)
+    size = group_size()
+    if k == 0:
+        sends, _, _ = raw_partner(d, 1)
+    else:
+        sends, group, _ = group_partner(d, group_strides()[k - 1])
+
+    @pl.when(sends)
     def _():
         lanes = slice(h * DEPTH, (h + 1) * DEPTH)
         keep = jnp.exp(offset[d, :, lanes])
@@ -141,20 +170,50 @@
         sent[k, d, h, DEPTH:, :] = jnp.broadcast_to(
             keep * before_keep[d, :, lanes], (16, DEPTH)
         ).astype(BF16)
-        scan_copy(k, d, h, sent, landed, p_send, p_recv).start()
+        if k == 0:
+            for j in range(size - 1, 0, -1):
+                exists, target, _ = raw_partner(d, j)
+
+                @pl.when(exists)
+                def _():
+                    scan_copy(j - 1, k, d, h, target, sent, landed, p_send, p_recv).start()
+        else:
+            for place in range(size - 1, -1, -1) if d == 0 else range(size):
+                target = group * size + place
+                scan_copy(size + k - 2, k, d, h, target, sent, landed, p_send, p_recv).start()
 
 
 def scan_close(k, d, h, sent, landed, before, before_keep, p_send, p_recv):
-    _, _, source = partner(d, strides()[k])
-
-    @pl.when(source)
-    def _():
-        scan_copy(k, d, h, sent, landed, p_send, p_recv).wait_recv()
-        lanes = slice(h * DEPTH, (h + 1) * DEPTH)
-        keep = before_keep[d, :, lanes]
-        early = landed[k, d, h].astype(F32)
-        before[d, h] = keep * early[:DEPTH] + before[d, h]
-        before_keep[d, :, lanes] = keep * early[DEPTH : DEPTH + 1]
+    size = group_size()
+    if k == 0:
+        arrivals = [(j - 1, *raw_partner(d, j)[1:]) for j in range(1, size)]
+    else:
+        arrivals = [(size + k - 2, 0, group_partner(d, group_strides()[k - 1])[2])]
+    for slot, target, gets in arrivals:
+        @pl.when(gets)
+        def _():
+            scan_copy(slot, k, d, h, target, sent, landed, p_send, p_recv).wait_recv()
+            lanes = slice(h * DEPTH, (h + 1) * DEPTH)
+            keep = before_keep[d, :, lanes]
+            early = landed[slot, d, h].astype(F32)
+            before[d, h] = keep * early[:DEPTH] + before[d, h]
+            before_keep[d, :, lanes] = keep * early[DEPTH : DEPTH + 1]
+
+
+def scan_drain(k, d, sent, landed, p_send, p_recv):
+    size = group_size()
+    if k == 0:
+        leaving = [(j - 1, raw_partner(d, j)[0], sent.at[0, d]) for j in range(1, size)]
+    else:
+        sends = group_partner(d, group_strides()[k - 1])[0]
+        leaving = [(size + k - 2, sends, landed.at[pl.ds(0, size // 2)])]
+    for slot, sends, block in leaving:
+        @pl.when(sends)
+        def _():
+            pltpu.make_async_remote_copy(
+                block, block, p_send.at[slot, d], p_recv.at[slot, d, 0],
+                device_id={"sp": 0}, device_id_type=MESH,
+            ).wait_send()
 
 
 def mixer_kernel(groups, *refs):
@@ -178,7 +237,7 @@
     subs = share // CHUNK
     features = 4 * width
     depth = wfull.shape[1] // 2
-    steps = len(strides())
+    steps = 1 + len(group_strides())
 
     own_w = [
         pltpu.make_async_copy(h_recur, wfull.at[me, pl.ds(0, depth)], l_sem.at[0]),
@@ -510,14 +569,7 @@
 
         for k in range(steps):
             for d in range(2):
-                exists, _, _ = partner(d, strides()[k])
-
-                @pl.when(exists)
-                def _():
-                    pltpu.make_async_remote_copy(
-                        sent.at[k, d], sent.at[k, d], p_send.at[k, d], p_recv.at[k, d, 0],
-                        device_id={"tp": sibling}, device_id_type=MESH,
-                    ).wait_send()
+                scan_drain(k, d, sent, landed, p_send, p_recv)
 
         pool_all.wait_send()
 
@@ -578,10 +630,8 @@
     fillers = [
         [late_last, ring_end] + [functools.partial(pool_away, r) for r in (1, 2, 3)],
         [lambda: pool_away(0), drain_gather],
-        [wide_pool],
     ]
-    first = 1 - lax.rem(lax.axis_index("sp"), 2)
-    rounds = [[] for _ in range(max(steps, 1))]
+    rounds = [[] for _ in range(steps)]
     for i, group in enumerate(fillers):
         rounds[min(i, len(rounds) - 1)].extend(group)
     for k in range(steps):
@@ -592,19 +642,14 @@
             for h in range(heads):
                 scan_start(0, 1, h, state, offset, *scan)
         for h in range(heads if k else 0):
-            for d in (first, 1 - first):
+            for d in range(2):
                 scan_close(k - 1, d, h, *scan)
                 scan_start(k, d, h, state, offset, *scan)
         for filler in rounds[k]:
             filler()
-    if not steps:
-        lax.fori_loop(0, count, descend, 0)
-        for filler in rounds[0]:
-            filler()
     for h in range(heads):
         for d in range(2):
-            if steps:
-                scan_close(steps - 1, d, h, *scan)
+            scan_close(steps - 1, d, h, *scan)
             lanes = slice(d * DEPTH, (d + 1) * DEPTH)
             keep = before_keep[d, :, h * DEPTH : (h + 1) * DEPTH]
             turned[h, :, lanes] = keep * turned[h, :, lanes] + before[d, h]
@@ -624,6 +669,7 @@
             jnp.concatenate([wfull[across, rows, lanes], wfull[opposite, rows, lanes]], axis=0),
         )
 
+    wide_pool()
     recur_wait(1, heads, heads).wait_recv()
     home = pl.ds(pl.multiple_of(me * share, share), share)
     for j in range(tiles):
@@ -661,9 +707,10 @@
     share = length // 4
     subs = share // CHUNK
     depth, out_width = w_out_recur.shape
-    steps = len(strides())
+    steps = 1 + len(group_strides())
     size = ring_size()
     events = size - 1
+    slots = group_size() - 1 + steps - 1
     dma = pltpu.SemaphoreType.DMA
     operands = (
         tokens, norm_gain[None, :], *weights, forget_gap, added_log_retention.T, initial_state,
@@ -705,7 +752,7 @@
             pltpu.VMEM((2, 1, columns), F32),
             pltpu.VMEM((length + 2 * RIM, columns), BF16),
             pltpu.VMEM((steps, 2, heads, DEPTH + 16, DEPTH), BF16),
-            pltpu.VMEM((steps, 2, heads, DEPTH + 16, DEPTH), BF16),
+            pltpu.VMEM((slots, 2, heads, DEPTH + 16, DEPTH), BF16),
             pltpu.VMEM((2, heads, DEPTH, DEPTH), F32),
             pltpu.VMEM((2, 1, columns), F32),
             pltpu.VMEM((heads, length, DEPTH), BF16),
@@ -717,7 +764,7 @@
             pltpu.VMEM((CHUNK, 1), F32),
             dma((10,)), dma((1,)), dma((1,)), dma((1,)), dma((count,)), dma((count,)),
             dma((1,)), dma((1,)), dma((events,)),
-            dma((steps, 2)), dma((steps, 2, heads)), dma((2,)), dma((2,)),
+            dma((slots, 2)), dma((slots, 2, heads)), dma((2,)), dma((2,)),
             dma((1,)), dma((1,)), dma((1,)), dma((heads + 1,)),
         ],
         compiler_params=pltpu.CompilerParams(

time: 57.1 us -> 54.1 us (0.947)
  Pallas kernels: 56 us -> 52.9 us
    pallas_call x1, Pallas kernels: 56 us -> 52.9 us  [shards(): pl.pallas_call(functools.partial(mixer_kernel, pool_mix.shape[0]), out_sh...]
where the time goes in v5:
time: 54.1 us; the launch traced here: 53.8 us
  Pallas kernels  52.9 us (98%)
  local copies, waits for them, and re-layouts  0.97 us (2%)
    pallas_call x1, Pallas kernels, shards(): pl.pallas_call(functools.partial(mixer_kernel, pool_mix.shape[0]), out_sh...  52.9 us

profile of v5, /device:TPU:1, one launch (start us, length us, event | category | flops | bytes accessed | tf_op | source)
XLA Modules:
  0.0 53.8 jit_solution(2901240318807431128)
XLA Ops:
  0.0 52.9 %mixer.1 = bf16[256,2048]{1,0:T(8,128)(2,1)S(1)} custom-call(bf16[1024,512]{1,0:T(8,128)(2,1)} %refs_0_.1, f32[1,2048]{1,0:T(1,128)} %bitcast.4, bf16[2048,256]{1,0:T(8,128)(2,1)} %refs_2_.1, bf16[2048,256]{1,0:T(8,128)(2,1)} %refs_3_.1, bf16[2048,256]{1,0:T(8,128)(2,1)} %refs_4_.1, bf16[2048,256]{1,0:T(8,128)(2,1)} %refs_5_.1, bf16[2048,256]{1,0:T(8,128)(2,1)} %refs_6_.1, ...), custom_call_target="tpu_custom_call" | custom-call | tf_op jit(solution)/shard_map/mixer/pallas_call | solution.py:723
  52.9 1.0 %copy.18 = bf16[256,2048]{1,0:T(8,128)(2,1)} copy(bf16[256,2048]{1,0:T(8,128)(2,1)S(1)} %mixer.1) | data formatting | bytes 2097152

commit v6 on v5

--- a/solution.py
+++ b/solution.py
@@ -74,8 +74,8 @@
     count = lax.axis_size("sp") // size
     above, below = group + stride < count, group >= stride
     if d == 0:
-        return above & (place == size - 1), group + stride, below
-    return below & (place == 0), group - stride, above
+        return above & (place >= size - 2), group + stride, below
+    return below & (place < 2), group - stride, above
 
 
 def ring_size():
@@ -111,7 +111,8 @@
     for stride in group_strides():
         for d in range(2):
             sends, _, gets = group_partner(d, stride)
-            source = (group - stride) * size + size - 1 if d == 0 else (group + stride) * size
+            source = (group - stride) * size + size - 2 if d == 0 else (group + stride) * size
+            source = source + lax.rem(place, 2)
 
             @pl.when(gets)
             def _():
@@ -119,7 +120,16 @@
                     barrier, inc=1, device_id={"sp": source}, device_id_type=MESH
                 )
 
-            number = number + jnp.where(sends, size, 0)
+            number = number + jnp.where(sends, size // 2, 0)
+    for d in range(2):
+        exists, target, _ = partner(d, 1)
+        outside = exists & (place == (size - 1 if d == 0 else 0))
+
+        @pl.when(outside)
+        def _():
+            pl.semaphore_signal(barrier, inc=1, device_id={"sp": target}, device_id_type=MESH)
+
+        number = number + jnp.where(outside, 1, 0)
     pl.semaphore_wait(barrier, number)
 
 
@@ -155,44 +165,84 @@
     )
 
 
-def scan_start(k, d, h, state, offset, sent, landed, before, before_keep, p_send, p_recv):
+def raw_sends(d):
+    size, (_, place), me = group_size(), group_place(), lax.axis_index("sp")
+    rows = []
+    for j in range(size - 1, 0, -1):
+        exists, target, _ = raw_partner(d, j)
+        rows.append((j - 1, exists, target, place + j >= size - 2 if d == 0 else place - j < 2))
+    if d == 0:
+        extra = (size - 1, place == size - 1, me - 1, place >= 0)
+    else:
+        extra = (size - 1, place == 0, me + 1, place >= 0)
+    return [extra] + rows
+
+
+def raw_start(d, h, state, offset, sent, landed, before, before_keep, p_send, p_recv):
+    lanes = slice(h * DEPTH, (h + 1) * DEPTH)
+    sent[0, d, h, :DEPTH, :] = state[d, h].astype(BF16)
+    sent[0, d, h, DEPTH:, :] = jnp.broadcast_to(
+        jnp.exp(offset[d, :, lanes]), (16, DEPTH)
+    ).astype(BF16)
+    for slot, exists, target, boundary in raw_sends(d):
+        @pl.when(exists & boundary)
+        def _():
+            scan_copy(slot, 0, d, h, target, sent, landed, p_send, p_recv).start()
+
+
+def raw_rest(d, h, sent, landed, before, before_keep, p_send, p_recv):
+    for slot, exists, target, boundary in raw_sends(d):
+        @pl.when(exists & jnp.logical_not(boundary))
+        def _():
+            scan_copy(slot, 0, d, h, target, sent, landed, p_send, p_recv).start()
+
+
+def total_start(k, d, h, state, offset, sent, landed, before, before_keep, p_send, p_recv):
+    size, (_, place) = group_size(), group_place()
+    sends, group, _ = group_partner(d, group_strides()[k - 1])
+    inner = place == (size - 2 if d == 0 else 1)
+    lanes = slice(h * DEPTH, (h + 1) * DEPTH)
+
+    def send(values, keep):
+        sent[k, d, h, :DEPTH, :] = values.astype(BF16)
+        sent[k, d, h, DEPTH:, :] = jnp.broadcast_to(keep, (16, DEPTH)).astype(BF16)
+        for pair in range(size // 2 - 1, -1, -1) if d == 0 else range(size // 2):
+            target = group * size + 2 * pair + lax.rem(place, 2)
+            scan_copy(size + k - 1, k, d, h, target, sent, landed, p_send, p_recv).start()
+
+    @pl.when(sends & jnp.logical_not(inner))
+    def _():
+        keep = jnp.exp(offset[d, :, lanes])
+        send(keep * before[d, h] + state[d, h], keep * before_keep[d, :, lanes])
+
+    @pl.when(sends & inner)
+    def _():
+        if k == 1:
+            scan_copy(size - 1, 0, d, h, 0, sent, landed, p_send, p_recv).wait_recv()
+        last = landed[size - 1, d, h].astype(F32)
+        keep = jnp.exp(offset[d, :, lanes])
+        last_keep = last[DEPTH : DEPTH + 1]
+        send(
+            last_keep * (keep * before[d, h] + state[d, h]) + last[:DEPTH],
+            last_keep * (keep * before_keep[d, :, lanes]),
+        )
+
+    if k == 1:
+        @pl.when(inner & jnp.logical_not(sends))
+        def _():
+            scan_copy(size - 1, 0, d, h, 0, sent, landed, p_send, p_recv).wait_recv()
+
+
+def scan_close(k, d, h, only, sent, landed, before, before_keep, p_send, p_recv):
     size = group_size()
     if k == 0:
-        sends, _, _ = raw_partner(d, 1)
+        arrivals = [(j - 1, raw_partner(d, j)[2]) for j in range(1, size)]
     else:
-        sends, group, _ = group_partner(d, group_strides()[k - 1])
-
-    @pl.when(sends)
-    def _():
-        lanes = slice(h * DEPTH, (h + 1) * DEPTH)
-        keep = jnp.exp(offset[d, :, lanes])
-        sent[k, d, h, :DEPTH, :] = (keep * before[d, h] + state[d, h]).astype(BF16)
-        sent[k, d, h, DEPTH:, :] = jnp.broadcast_to(
-            keep * before_keep[d, :, lanes], (16, DEPTH)
-        ).astype(BF16)
-        if k == 0:
-            for j in range(size - 1, 0, -1):
-                exists, target, _ = raw_partner(d, j)
-
-                @pl.when(exists)
-                def _():
-                    scan_copy(j - 1, k, d, h, target, sent, landed, p_send, p_recv).start()
-        else:
-            for place in range(size - 1, -1, -1) if d == 0 else range(size):
-                target = group * size + place
-                scan_copy(size + k - 2, k, d, h, target, sent, landed, p_send, p_recv).start()
-
-
-def scan_close(k, d, h, sent, landed, before, before_keep, p_send, p_recv):
-    size = group_size()
-    if k == 0:
-        arrivals = [(j - 1, *raw_partner(d, j)[1:]) for j in range(1, size)]
-    else:
-        arrivals = [(size + k - 2, 0, group_partner(d, group_strides()[k - 1])[2])]
-    for slot, target, gets in arrivals:
-        @pl.when(gets)
-        def _():
-            scan_copy(slot, k, d, h, target, sent, landed, p_send, p_recv).wait_recv()
+        arrivals = [(size + k - 1, group_partner(d, group_strides()[k - 1])[2])]
+    for slot, gets in arrivals:
+        @pl.when(gets & only)
+        def _():
+            scan_copy(slot, k, d, h, 0, sent, landed, p_send, p_recv).wait_recv()
             lanes = slice(h * DEPTH, (h + 1) * DEPTH)
             keep = before_keep[d, :, lanes]
             early = landed[slot, d, h].astype(F32)
@@ -203,10 +253,10 @@
 def scan_drain(k, d, sent, landed, p_send, p_recv):
     size = group_size()
     if k == 0:
-        leaving = [(j - 1, raw_partner(d, j)[0], sent.at[0, d]) for j in range(1, size)]
+        leaving = [(slot, exists, sent.at[0, d]) for slot, exists, _, _ in raw_sends(d)]
     else:
         sends = group_partner(d, group_strides()[k - 1])[0]
-        leaving = [(size + k - 2, sends, landed.at[pl.ds(0, size // 2)])]
+        leaving = [(size + k - 1, sends, landed.at[pl.ds(0, size // 4)])]
     for slot, sends, block in leaving:
         @pl.when(sends)
         def _():
@@ -574,8 +624,6 @@
         pool_all.wait_send()
 
     def late_last():
-        late_pool(count - 1)
-        edge_start(0, length, padded, e_send, e_recv)
         late(count - 1)
         local(count - 1)
 
@@ -627,29 +675,48 @@
             recur_copy(k, h).start()
 
     scan = (sent, landed, before, before_keep, p_send, p_recv)
+    place_in_group = group_place()[1]
+    always = place_in_group >= 0
+    leads = (place_in_group >= group_size() // 2, place_in_group < group_size() // 2)
+
+    def close_rest():
+        for h in range(heads):
+            for d in range(2):
+                scan_close(0, d, h, leads[1 - d] if steps > 1 else always, *scan)
+
     fillers = [
-        [late_last, ring_end] + [functools.partial(pool_away, r) for r in (1, 2, 3)],
-        [lambda: pool_away(0), drain_gather],
+        [late_last, ring_end] + [functools.partial(pool_away, r) for r in (1, 2, 3)]
+        + ([] if steps > 1 else [lambda: pool_away(0), close_rest, drain_gather]),
+        [close_rest, drain_gather] if steps > 1 else [],
     ]
     rounds = [[] for _ in range(steps)]
     for i, group in enumerate(fillers):
         rounds[min(i, len(rounds) - 1)].extend(group)
     for k in range(steps):
         if k == 0:
+            raw_start(0, 0, state, offset, *scan)
+            lax.fori_loop(0, count, descend, 0)
+            raw_start(1, 0, state, offset, *scan)
+            late_pool(count - 1)
+            edge_start(0, length, padded, e_send, e_recv)
+            for h in range(1, heads):
+                for d in range(2):
+                    raw_start(d, h, state, offset, *scan)
             for h in range(heads):
-                scan_start(0, 0, h, state, offset, *scan)
-            lax.fori_loop(0, count, descend, 0)
-            for h in range(heads):
-                scan_start(0, 1, h, state, offset, *scan)
+                for d in range(2):
+                    raw_rest(d, h, *scan)
         for h in range(heads if k else 0):
             for d in range(2):
-                scan_close(k - 1, d, h, *scan)
-                scan_start(k, d, h, state, offset, *scan)
+                scan_close(k - 1, d, h, leads[d] if k == 1 else always, *scan)
+            for d in range(2):
+                total_start(k, d, h, state, offset, *scan)
+            if k == 1 and h == 0:
+                pool_away(0)
         for filler in rounds[k]:
             filler()
     for h in range(heads):
         for d in range(2):
-            scan_close(steps - 1, d, h, *scan)
+            scan_close(steps - 1, d, h, always, *scan)
             lanes = slice(d * DEPTH, (d + 1) * DEPTH)
             keep = before_keep[d, :, h * DEPTH : (h + 1) * DEPTH]
             turned[h, :, lanes] = keep * turned[h, :, lanes] + before[d, h]
@@ -710,7 +777,7 @@
     steps = 1 + len(group_strides())
     size = ring_size()
     events = size - 1
-    slots = group_size() - 1 + steps - 1
+    slots = group_size() + steps - 1
     dma = pltpu.SemaphoreType.DMA
     operands = (
         tokens, norm_gain[None, :], *weights, forget_gap, added_log_retention.T, initial_state,

time: 54.1 us -> 53.2 us (0.983)
  Pallas kernels: 52.9 us -> 52.1 us
    pallas_call x1, Pallas kernels: 52.9 us -> 52.1 us  [shards(): pl.pallas_call(functools.partial(mixer_kernel, pool_mix.shape[0]), out_sh...]
where the time goes in v6:
time: 53.2 us; the launch traced here: 53.1 us
  Pallas kernels  52.1 us (98%)
  local copies, waits for them, and re-layouts  0.97 us (2%)
    pallas_call x1, Pallas kernels, shards(): pl.pallas_call(functools.partial(mixer_kernel, pool_mix.shape[0]), out_sh...  52.1 us

profile of v6, /device:TPU:1, one launch (start us, length us, event | category | flops | bytes accessed | tf_op | source)
XLA Modules:
  0.0 53.1 jit_solution(17108209222565388257)
XLA Ops:
  0.0 52.1 %mixer.1 = bf16[256,2048]{1,0:T(8,128)(2,1)S(1)} custom-call(bf16[1024,512]{1,0:T(8,128)(2,1)} %refs_0_.1, f32[1,2048]{1,0:T(1,128)} %bitcast.4, bf16[2048,256]{1,0:T(8,128)(2,1)} %refs_2_.1, bf16[2048,256]{1,0:T(8,128)(2,1)} %refs_3_.1, bf16[2048,256]{1,0:T(8,128)(2,1)} %refs_4_.1, bf16[2048,256]{1,0:T(8,128)(2,1)} %refs_5_.1, bf16[2048,256]{1,0:T(8,128)(2,1)} %refs_6_.1, ...), custom_call_target="tpu_custom_call" | custom-call | tf_op jit(solution)/shard_map/mixer/pallas_call | solution.py:790
  52.1 1.0 %copy.18 = bf16[256,2048]{1,0:T(8,128)(2,1)} copy(bf16[256,2048]{1,0:T(8,128)(2,1)S(1)} %mixer.1) | data formatting | bytes 2097152

commit v7 on v6

--- a/solution.py
+++ b/solution.py
@@ -480,21 +480,23 @@
     def project(j, x, scale, at):
         return ((acc[j, at, :] + dot(x, wide[j, depth_of(far), :])) * scale).astype(BF16)
 
-    def late_pool(c):
-        rows = project(5, kept_x[...], kept_scale[...], piece(c))
+    def late_pool(c, rows=None):
+        slot = lax.rem(c, 2)
+        if rows is None:
+            rows = project(5, kept_x[slot], kept_scale[slot], piece(c))
         padded[pl.ds(pl.multiple_of(c * CHUNK + RIM, RIM), CHUNK), :] = rows
 
-    def late(c):
-        at, x, scale = piece(c), kept_x[...], kept_scale[...]
-        query_pre[at, :] = project(0, x, scale, at)
-        gate = project(4, x, scale, at).astype(F32)
+    def late(c, again=None):
+        at, x, scale = piece(c), kept_x[lax.rem(c, 2)], kept_scale[lax.rem(c, 2)]
+        again = again or (lambda j: project(j, x, scale, at))
+        query_pre[at, :] = again(0)
+        gate = again(4).astype(F32)
         gated[at, :] = head_gain[...] / (1.0 + jnp.exp(-gate))
 
     def step(i, _):
         at = piece(i)
         crossing(i).wait_recv()
         relay(i).start()
-
         @pl.when(i > 0)
         def _():
             late_pool(i - 1)
@@ -512,9 +514,44 @@
         relay(i).wait_recv()
         x, squares = normed(far, at)
         scale = lax.rsqrt((square[at, :] + squares) / features + EPSILON)
-
-        kept_x[...], kept_scale[...] = x, scale
-        pre_f, pre_b, values = (project(j, x, scale, at) for j in (1, 2, 3))
+        kept_x[lax.rem(i, 2)], kept_scale[lax.rem(i, 2)] = x, scale
+        advance(i, *(project(j, x, scale, at) for j in (1, 2, 3)))
+        return 0
+
+    def last_step():
+        i = count - 1
+        at, slot = piece(i), i % 2
+
+        def half(owner):
+            x = held[owner, at, :].astype(F32)
+            lanes = pl.ds(pl.multiple_of(owner * width, width), width)
+            part = (x * gain[:, lanes]).astype(BF16)
+            inside = pl.ds(pl.multiple_of((owner - far) * width, width), width)
+            kept_x[slot, :, inside] = part
+            return part, jnp.sum(x * x, axis=1, keepdims=True)
+
+        def rows_of_w(owner):
+            return pl.ds(pl.multiple_of(owner * width, width), width)
+
+        crossing(i).wait_recv()
+        relay(i).start()
+        x, squares = half(across)
+        square[at, :] = square[at, :] + squares
+        for j in range(6):
+            acc[j, at, :] = acc[j, at, :] + dot(x, wide[j, rows_of_w(across), :])
+        relay(i).wait_recv()
+        x, squares = half(opposite)
+        scale = lax.rsqrt((square[at, :] + squares) / features + EPSILON)
+        kept_scale[slot] = scale
+
+        def project_half(j):
+            y = acc[j, at, :] + dot(x, wide[j, rows_of_w(opposite), :])
+            return (y * scale).astype(BF16)
+
+        advance(i, *(project_half(j) for j in (1, 2, 3)))
+
+    def advance(i, pre_f, pre_b, values):
+        at = piece(i)
         value[at, :] = values
         enter_f, run_f = gates(pre_f.astype(F32), gap[0:1, :], lower_2)
         enter_b, run_b = gates(pre_b.astype(F32), gap[1:2, :], upper_2)
@@ -538,9 +575,9 @@
             chunk_state[i, h] = ends[:, DEPTH:]
             chunk_keep[i, :, lanes] = close_b[:, lanes] + b_end
             offset[0, :, lanes] = offset[0, :, lanes] + total_f
-        return 0
-
-    lax.fori_loop(0, count, step, 0)
+
+    lax.fori_loop(0, count - 1, step, 0)
+    last_step()
 
     def descend(i, _):
         c = count - 1 - i
@@ -598,7 +635,7 @@
             pool_copy(r).start()
 
     def ring_end():
-        for e in range(count - 1, events):
+        for e in range(count - 2, events):
             ring_turn(e)
 
     def drain_gather():
@@ -623,8 +660,25 @@
 
         pool_all.wait_send()
 
+    def half_again(j):
+        at = piece(count - 1)
+        owner = pl.ds(pl.multiple_of(opposite * width, width), width)
+        inside = pl.ds(pl.multiple_of((opposite - far) * width, width), width)
+        slot = (count - 1) % 2
+        y = acc[j, at, :] + dot(kept_x[slot, :, inside], wide[j, owner, :])
+        return (y * kept_scale[slot]).astype(BF16)
+
     def late_last():
-        late(count - 1)
+        late_pool(count - 2)
+        late(count - 2)
+        local(count - 2)
+        for h in range(1, heads):
+            for d in range(2):
+                raw_start(d, h, state, offset, *scan)
+        for h in range(heads):
+            for d in range(2):
+                raw_rest(d, h, *scan)
+        late(count - 1, half_again)
         local(count - 1)
 
     tile = 512
@@ -661,10 +715,10 @@
             device_id={"tp": there}, device_id_type=MESH,
         )
 
-    def recur_wait(owners, count, h):
-        rows = taken.at[pl.ds(0, owners), pl.ds(0, count)]
+    def recur_wait(owners, count, sem):
+        block = taken.at[pl.ds(0, owners), pl.ds(0, count)]
         return pltpu.make_async_remote_copy(
-            rows, rows, c_send.at[0], c_recv.at[h],
+            block, block, c_send.at[0], c_recv.at[sem],
             device_id={"tp": sibling}, device_id_type=MESH,
         )
 
@@ -697,14 +751,8 @@
             raw_start(0, 0, state, offset, *scan)
             lax.fori_loop(0, count, descend, 0)
             raw_start(1, 0, state, offset, *scan)
-            late_pool(count - 1)
+            late_pool(count - 1, half_again(5))
             edge_start(0, length, padded, e_send, e_recv)
-            for h in range(1, heads):
-                for d in range(2):
-                    raw_start(d, h, state, offset, *scan)
-            for h in range(heads):
-                for d in range(2):
-                    raw_rest(d, h, *scan)
         for h in range(heads if k else 0):
             for d in range(2):
                 scan_close(k - 1, d, h, leads[d] if k == 1 else always, *scan)
@@ -748,16 +796,15 @@
             all_heads(lambda h: taken[sibling, h]), wfull[sibling, :depth, lanes]
         )
     drain_scan()
-    for h in range(heads):
+    for h in range(heads - 1):
         recur_wait(1, 2, h).wait_recv()
         for j in range(tiles):
             lanes = slice(j * tile, (j + 1) * tile)
-            y = total[:, lanes] + far_part(h, lanes)
-            if h == heads - 1:
-                out[:, lanes] = y.astype(BF16)
-            else:
-                total[:, lanes] = y
-
+            total[:, lanes] = total[:, lanes] + far_part(h, lanes)
+    recur_wait(1, 2, heads - 1).wait_recv()
+    for j in range(tiles):
+        lanes = slice(j * tile, (j + 1) * tile)
+        out[:, lanes] = (total[:, lanes] + far_part(heads - 1, lanes)).astype(BF16)
     recur_wait(3, heads, 0).wait_send()
 
 
@@ -827,8 +874,8 @@
             pltpu.VMEM((4, share, columns), BF16),
             pltpu.VMEM((4, share, columns), BF16),
             pltpu.VMEM((share, out_width), F32),
-            pltpu.VMEM((CHUNK, 2 * width), BF16),
-            pltpu.VMEM((CHUNK, 1), F32),
+            pltpu.VMEM((2, CHUNK, 2 * width), BF16),
+            pltpu.VMEM((2, CHUNK, 1), F32),
             dma((10,)), dma((1,)), dma((1,)), dma((1,)), dma((count,)), dma((count,)),
             dma((1,)), dma((1,)), dma((events,)),
             dma((slots, 2)), dma((slots, 2, heads)), dma((2,)), dma((2,)),

time: 53.2 us -> 52.9 us (level)
  no operation moved by 1% of the time
where the time goes in v7:
time: 52.9 us; the launch traced here: 52.8 us
  Pallas kernels  51.8 us (98%)
  local copies, waits for them, and re-layouts  0.97 us (2%)
    pallas_call x1, Pallas kernels, shards(): pl.pallas_call(functools.partial(mixer_kernel, pool_mix.shape[0]), out_sh...  51.8 us

profile of v7, /device:TPU:1, one launch (start us, length us, event | category | flops | bytes accessed | tf_op | source)
XLA Modules:
  0.0 52.8 jit_solution(2042885085938900307)
XLA Ops:
  0.0 51.8 %mixer.1 = bf16[256,2048]{1,0:T(8,128)(2,1)S(1)} custom-call(bf16[1024,512]{1,0:T(8,128)(2,1)} %refs_0_.1, f32[1,2048]{1,0:T(1,128)} %bitcast.4, bf16[2048,256]{1,0:T(8,128)(2,1)} %refs_2_.1, bf16[2048,256]{1,0:T(8,128)(2,1)} %refs_3_.1, bf16[2048,256]{1,0:T(8,128)(2,1)} %refs_4_.1, bf16[2048,256]{1,0:T(8,128)(2,1)} %refs_5_.1, bf16[2048,256]{1,0:T(8,128)(2,1)} %refs_6_.1, ...), custom_call_target="tpu_custom_call" | custom-call | tf_op jit(solution)/shard_map/mixer/pallas_call | solution.py:837
  51.8 1.0 %copy.18 = bf16[256,2048]{1,0:T(8,128)(2,1)} copy(bf16[256,2048]{1,0:T(8,128)(2,1)S(1)} %mixer.1) | data formatting | bytes 2097152

commit v8 on v7

--- a/solution.py
+++ b/solution.py
@@ -160,7 +160,8 @@
 
 def scan_copy(slot, k, d, h, target, sent, landed, p_send, p_recv):
     return pltpu.make_async_remote_copy(
-        sent.at[k, d, h], landed.at[slot, d, h], p_send.at[slot, d], p_recv.at[slot, d, h],
+        sent.at[k, d, h], landed.at[slot, d, h],
+        p_send.at[2 * k - 1 + d if k else 0], p_recv.at[k, d, h],
         device_id={"sp": target}, device_id_type=MESH,
     )
 
@@ -217,8 +218,6 @@
 
     @pl.when(sends & inner)
     def _():
-        if k == 1:
-            scan_copy(size - 1, 0, d, h, 0, sent, landed, p_send, p_recv).wait_recv()
         last = landed[size - 1, d, h].astype(F32)
         keep = jnp.exp(offset[d, :, lanes])
         last_keep = last[DEPTH : DEPTH + 1]
@@ -227,43 +226,62 @@
             last_keep * (keep * before_keep[d, :, lanes]),
         )
 
-    if k == 1:
-        @pl.when(inner & jnp.logical_not(sends))
-        def _():
-            scan_copy(size - 1, 0, d, h, 0, sent, landed, p_send, p_recv).wait_recv()
+
+def scan_wait(block, send, recv):
+    return pltpu.make_async_remote_copy(
+        block, block, send, recv, device_id={"sp": 0}, device_id_type=MESH
+    )
 
 
 def scan_close(k, d, h, only, sent, landed, before, before_keep, p_send, p_recv):
-    size = group_size()
-    if k == 0:
-        arrivals = [(j - 1, raw_partner(d, j)[2]) for j in range(1, size)]
-    else:
-        arrivals = [(size + k - 1, group_partner(d, group_strides()[k - 1])[2])]
-    for slot, gets in arrivals:
-        @pl.when(gets & only)
-        def _():
-            scan_copy(slot, k, d, h, 0, sent, landed, p_send, p_recv).wait_recv()
-            lanes = slice(h * DEPTH, (h + 1) * DEPTH)
-            keep = before_keep[d, :, lanes]
-            early = landed[slot, d, h].astype(F32)
-            before[d, h] = keep * early[:DEPTH] + before[d, h]
-            before_keep[d, :, lanes] = keep * early[DEPTH : DEPTH + 1]
-
-
-def scan_drain(k, d, sent, landed, p_send, p_recv):
-    size = group_size()
-    if k == 0:
-        leaving = [(slot, exists, sent.at[0, d]) for slot, exists, _, _ in raw_sends(d)]
-    else:
-        sends = group_partner(d, group_strides()[k - 1])[0]
-        leaving = [(size + k - 1, sends, landed.at[pl.ds(0, size // 4)])]
-    for slot, sends, block in leaving:
+    size, (_, place) = group_size(), group_place()
+
+    def add(slot):
+        lanes = slice(h * DEPTH, (h + 1) * DEPTH)
+        keep = before_keep[d, :, lanes]
+        early = landed[slot, d, h].astype(F32)
+        before[d, h] = keep * early[:DEPTH] + before[d, h]
+        before_keep[d, :, lanes] = keep * early[DEPTH : DEPTH + 1]
+
+    def wait(block):
+        scan_wait(block, p_send.at[0], p_recv.at[k, d, h]).wait_recv()
+
+    if k:
+        @pl.when(group_partner(d, group_strides()[k - 1])[2] & only)
+        def _():
+            wait(landed.at[0, d, h])
+            add(size + k - 1)
+
+        return
+    boundary = place >= size - 2 if d == 0 else place < 2
+
+    @pl.when(only & boundary)
+    def _():
+        wait(landed.at[pl.ds(0, size - 1), d, h])
+        for j in range(1, size):
+            pl.when(raw_partner(d, j)[2])(functools.partial(add, j - 1))
+
+    @pl.when(only & jnp.logical_not(boundary) & raw_partner(d, 1)[2])
+    def _():
+        wait(landed.at[0, d, h])
+        add(0)
+
+
+def scan_drain(steps, landed, p_send, p_recv):
+    size, (_, place) = group_size(), group_place()
+    outer = (place == 0) | (place == size - 1)
+    leaving = [
+        (0, outer, landed.at[pl.ds(0, size // 2)]),
+        (0, jnp.logical_not(outer), landed.at[pl.ds(0, size - 1), 0]),
+    ]
+    for k in range(1, steps):
+        for d in range(2):
+            sends = group_partner(d, group_strides()[k - 1])[0]
+            leaving.append((2 * k - 1 + d, sends, landed.at[pl.ds(0, size // 4)]))
+    for index, sends, block in leaving:
         @pl.when(sends)
         def _():
-            pltpu.make_async_remote_copy(
-                block, block, p_send.at[slot, d], p_recv.at[slot, d, 0],
-                device_id={"sp": 0}, device_id_type=MESH,
-            ).wait_send()
+            scan_wait(block, p_send.at[index], p_recv.at[0, 0, 0]).wait_send()
 
 
 def mixer_kernel(groups, *refs):
@@ -579,16 +597,19 @@
     lax.fori_loop(0, count - 1, step, 0)
     last_step()
 
-    def descend(i, _):
-        c = count - 1 - i
-        offsets[1, c] = offset[1]
-        for h in range(heads):
-            lanes = slice(h * DEPTH, (h + 1) * DEPTH)
+    def descend(h):
+        lanes = slice(h * DEPTH, (h + 1) * DEPTH)
+
+        def one(i, _):
+            c = count - 1 - i
+            offsets[1, c, :, lanes] = offset[1, :, lanes]
             starts[c, h, :, DEPTH:] = state[1, h]
             keep = chunk_keep[c, :, lanes]
             state[1, h] = jnp.exp(keep) * state[1, h] + chunk_state[c, h]
             offset[1, :, lanes] = offset[1, :, lanes] + keep
-        return 0
+            return 0
+
+        lax.fori_loop(0, count, one, 0)
 
     window = jnp.left_shift(jnp.int32(2), lax.axis_index("tp") * groups)
     sequence, first_row = length * lax.axis_size("sp"), lax.axis_index("sp") * length
@@ -654,10 +675,7 @@
             def _():
                 edge_copy(d, length, padded, e_send, e_recv).wait_send()
 
-        for k in range(steps):
-            for d in range(2):
-                scan_drain(k, d, sent, landed, p_send, p_recv)
-
+        scan_drain(steps, landed, p_send, p_recv)
         pool_all.wait_send()
 
     def half_again(j):
@@ -749,8 +767,10 @@
     for k in range(steps):
         if k == 0:
             raw_start(0, 0, state, offset, *scan)
-            lax.fori_loop(0, count, descend, 0)
+            descend(0)
             raw_start(1, 0, state, offset, *scan)
+            for h in range(1, heads):
+                descend(h)
             late_pool(count - 1, half_again(5))
             edge_start(0, length, padded, e_send, e_recv)
         for h in range(heads if k else 0):
@@ -878,7 +898,7 @@
             pltpu.VMEM((2, CHUNK, 1), F32),
             dma((10,)), dma((1,)), dma((1,)), dma((1,)), dma((count,)), dma((count,)),
             dma((1,)), dma((1,)), dma((events,)),
-            dma((slots, 2)), dma((slots, 2, heads)), dma((2,)), dma((2,)),
+            dma((2 * steps - 1,)), dma((steps, 2, heads)), dma((2,)), dma((2,)),
             dma((1,)), dma((1,)), dma((1,)), dma((heads + 1,)),
         ],
         compiler_params=pltpu.CompilerParams(

time: 52.9 us -> 52.8 us (level)
  no operation moved by 1% of the time
where the time goes in v8:
time: 52.8 us; the launch traced here: 52.7 us
  Pallas kernels  51.7 us (98%)
  local copies, waits for them, and re-layouts  0.97 us (2%)
    pallas_call x1, Pallas kernels, shards(): pl.pallas_call(functools.partial(mixer_kernel, pool_mix.shape[0]), out_sh...  51.7 us

profile of v8, /device:TPU:1, one launch (start us, length us, event | category | flops | bytes accessed | tf_op | source)
XLA Modules:
  0.0 52.7 jit_solution(14602688431538379217)
XLA Ops:
  0.0 51.7 %mixer.1 = bf16[256,2048]{1,0:T(8,128)(2,1)S(1)} custom-call(bf16[1024,512]{1,0:T(8,128)(2,1)} %refs_0_.1, f32[1,2048]{1,0:T(1,128)} %bitcast.4, bf16[2048,256]{1,0:T(8,128)(2,1)} %refs_2_.1, bf16[2048,256]{1,0:T(8,128)(2,1)} %refs_3_.1, bf16[2048,256]{1,0:T(8,128)(2,1)} %refs_4_.1, bf16[2048,256]{1,0:T(8,128)(2,1)} %refs_5_.1, bf16[2048,256]{1,0:T(8,128)(2,1)} %refs_6_.1, ...), custom_call_target="tpu_custom_call" | custom-call | tf_op jit(solution)/shard_map/mixer/pallas_call | solution.py:857
  51.7 1.0 %copy.18 = bf16[256,2048]{1,0:T(8,128)(2,1)} copy(bf16[256,2048]{1,0:T(8,128)(2,1)S(1)} %mixer.1) | data formatting | bytes 2097152

commit v9 on v8

--- a/solution.py
+++ b/solution.py
@@ -778,7 +778,7 @@
                 scan_close(k - 1, d, h, leads[d] if k == 1 else always, *scan)
             for d in range(2):
                 total_start(k, d, h, state, offset, *scan)
-            if k == 1 and h == 0:
+            if k == 1 and h == heads - 1:
                 pool_away(0)
         for filler in rounds[k]:
             filler()

time: 52.8 us -> 53.7 us (1.017)
  Pallas kernels: 51.7 us -> 52.6 us
    pallas_call x1, Pallas kernels: 51.7 us -> 52.6 us  [shards(): pl.pallas_call(functools.partial(mixer_kernel, pool_mix.shape[0]), out_sh...]
where the time goes in v9:
time: 53.7 us; the launch traced here: 53.6 us
  Pallas kernels  52.6 us (98%)
  local copies, waits for them, and re-layouts  0.97 us (2%)
    pallas_call x1, Pallas kernels, shards(): pl.pallas_call(functools.partial(mixer_kernel, pool_mix.shape[0]), out_sh...  52.6 us

profile of v9, /device:TPU:1, one launch (start us, length us, event | category | flops | bytes accessed | tf_op | source)
XLA Modules:
  0.0 53.6 jit_solution(14648185911857545291)
XLA Ops:
  0.0 52.6 %mixer.1 = bf16[256,2048]{1,0:T(8,128)(2,1)S(1)} custom-call(bf16[1024,512]{1,0:T(8,128)(2,1)} %refs_0_.1, f32[1,2048]{1,0:T(1,128)} %bitcast.4, bf16[2048,256]{1,0:T(8,128)(2,1)} %refs_2_.1, bf16[2048,256]{1,0:T(8,128)(2,1)} %refs_3_.1, bf16[2048,256]{1,0:T(8,128)(2,1)} %refs_4_.1, bf16[2048,256]{1,0:T(8,128)(2,1)} %refs_5_.1, bf16[2048,256]{1,0:T(8,128)(2,1)} %refs_6_.1, ...), custom_call_target="tpu_custom_call" | custom-call | tf_op jit(solution)/shard_map/mixer/pallas_call | solution.py:857
  52.6 1.0 %copy.18 = bf16[256,2048]{1,0:T(8,128)(2,1)} copy(bf16[256,2048]{1,0:T(8,128)(2,1)S(1)} %mixer.1) | data formatting | bytes 2097152
